TPU v7x, 512 devices: a whole 4x4x16 slice. The times are simulated.
512 devices in a mesh: sp: 64 (over z, y), tp: 8 (over x, core).
Axes of the slice: x: 4, y: 4, z: 16, core: 2. Of those that a mesh axis runs over, the one named last changes fastest.
Arguments:
- tokens: bfloat16 [8192, 2048], P('sp', 'tp'), may hold values from -6 to 6
- norm_gain: float32 [2048], replicated, may hold values from 0.1 to 1.9
- w_value: bfloat16 [2048, 2048], P('sp', 'tp'), may hold values from -0.125 to 0.125
- w_gate: bfloat16 [2048, 2048], P('sp', 'tp'), may hold values from -0.125 to 0.125
- conv_taps: bfloat16 [31, 2048], P(None, 'tp'), may hold values from -1 to 1
- conv_gain: float32 [2048], P('tp'), may hold values from 0.1 to 1.9
- w_query: bfloat16 [2048, 3072], P(None, 'tp'), may hold values from -5.303301 to 5.303301
- latent_down_weight: bfloat16 [2048, 512], P('sp'), may hold values from -0.125 to 0.125
- latent_norm_gain: float32 [512], replicated, may hold values from 0.1 to 1.9
- w_rope_key: bfloat16 [2048, 64], P('sp'), may hold values from -0.125 to 0.125
- key_up_weight: bfloat16 [512, 2048], P(None, 'tp'), may hold values from -0.5 to 0.5
- value_up_weight: bfloat16 [512, 2048], P(None, 'tp'), may hold values from -0.25 to 0.25
- w_merge_conv: bfloat16 [2048, 2048], P('tp'), may hold values from -0.09375 to 0.09375
- w_merge_attn: bfloat16 [2048, 2048], P('tp'), may hold values from -0.28125 to 0.28125
Outputs:
- merged: bfloat16 [8192, 2048], P(('sp', 'tp'))
- log_sums: float32 [8192, 16], P('sp', 'tp')
All inputs are finite; a program needn't handle non-finite values.
Results may differ from a plain program's by a relative error of at most 0.025.
The roundings to bfloat16 on the way count: a program that leaves them out, or rounds other values in their place, can miss the bound.
Values may be sent and summed in bfloat16 or wider, within the bound.
A program may use at most 64 MiB of HBM per device.

v0:
```python
import jax
import jax.numpy as jnp
from jax import lax
from jax.sharding import Mesh
from jax.sharding import PartitionSpec as P

PLAIN_QK_WIDTH = 128
QK_ROPE = 64
VALUE_HEAD_WIDTH = 128
TP = ("tp_0", "tp_1")
SP_TP = ("sp", "tp_0", "tp_1")


epsilon = 1e-06
rope_base = 10000.0
masked_score = -1e30


def piece_ends(length, count):
    step = length // count
    if step >= 8:
        step -= step % 8
    return [step * k for k in range(1, count)]


def all_blocks(shard, axes, order):
    parts = shard[None]
    for k in order:
        parts = lax.all_gather(parts, axes[k], axis=0, tiled=True)
    current = [lax.axis_size(axes[k]) for k in reversed(order)]
    parts = parts.reshape(*current, *shard.shape)
    turned = sorted(range(len(order)), key=lambda place: order[len(order) - 1 - place])
    return parts.transpose(*turned, *range(len(order), parts.ndim)).reshape(-1, *shard.shape)


def laid_out(parts, dim):
    lengths = list(parts.shape[1:])
    lengths[dim] *= parts.shape[0]
    return jnp.moveaxis(parts, 0, dim).reshape(lengths)


def spread_gather(shard, axes, dim):
    widest = max(range(max(1, shard.ndim - 1)), key=lambda d: shard.shape[d])
    count, done = (len(axes), [])
    for leading, share in enumerate(
        jnp.split(shard, piece_ends(shard.shape[widest], count), axis=widest)
    ):
        if share.size:
            order = [(leading - k) % count for k in range(count)]
            done.append(all_blocks(share, axes, order))
    return laid_out(jnp.concatenate(done, axis=widest + 1), dim)


def side_by_side(arrays, axis, dim, along):
    both = jnp.concatenate(arrays, axis=along)
    result, at, done = (lax.all_gather(both, axis, axis=dim, tiled=True), 0, [])
    for a in arrays:
        done.append(lax.slice_in_dim(result, at, at + a.shape[along], axis=along))
        at += a.shape[along]
    return tuple(done)


def passed_along(block, axis, distance):
    devices = range(lax.axis_size(axis))
    route = [(i - distance, i) for i in devices if i - distance in devices]
    return lax.ppermute(block, axis, route)


def sent_to_all(shard, axis):
    copies = jnp.broadcast_to(shard, (lax.axis_size(axis), *shard.shape))
    return lax.all_to_all(copies, axis, split_axis=0, concat_axis=0, tiled=True)


def of_everyone(shard, axis):
    return sent_to_all(shard, axis).sum(axis=0)


def packed_total(arrays, axis):
    ravelled, at, done = (jnp.concatenate([a.reshape(-1) for a in arrays]), 0, [])
    subtotal = of_everyone(ravelled, axis)
    for a in arrays:
        done.append(subtotal[at : at + a.size].reshape(a.shape))
        at += a.size
    return tuple(done)


def split_up(shard, dim, count):
    before, after = (shard.shape[:dim], shard.shape[dim + 1 :])
    return jnp.moveaxis(shard.reshape(*before, count, -1, *after), dim, 0)


def summed_on_arrival(shard, axis, dim):
    count = lax.axis_size(axis)
    parts = lax.all_to_all(split_up(shard, dim, count), axis, 0, 0, tiled=True)
    return jnp.sum(parts.astype(jnp.float32), axis=0)


def angles_at(positions, width):
    inverse = rope_base ** (-2.0 * jnp.arange(width // 2, dtype=jnp.float32) / width)
    return positions[:, None] * inverse[None, :]


def rotate(halves, angle):
    middle = halves.shape[-1] // 2
    first, second = (halves[..., :middle], halves[..., middle:])
    cosine, sine = (jnp.cos(angle), jnp.sin(angle))
    return jnp.concatenate(
        [first * cosine - second * sine, first * sine + second * cosine], axis=-1
    )


def local(
    tokens,
    norm_gain,
    w_value,
    w_gate,
    conv_taps,
    conv_gain,
    w_query,
    latent_down_weight,
    latent_norm_gain,
    w_rope_key,
    key_up_weight,
    value_up_weight,
    w_merge_conv,
    w_merge_attn,
):
    row_count = tokens.shape[0]
    tp_count = lax.axis_size(TP)
    gathered = spread_gather(tokens, TP, 1)
    features = gathered.astype(jnp.float32)
    normed = (
        features
        * lax.rsqrt(jnp.mean(features * features, axis=-1, keepdims=True) + epsilon)
        * norm_gain
    ).astype(jnp.bfloat16)
    first_row = lax.axis_index("sp") * row_count
    query_index = first_row + jnp.arange(row_count, dtype=jnp.int32)
    pieces = side_by_side((w_value, w_gate, latent_down_weight, w_rope_key), "sp", 0, 1)
    value_pre = jnp.dot(normed, pieces[0], preferred_element_type=jnp.float32)
    gate_pre = jnp.dot(normed, pieces[1], preferred_element_type=jnp.float32)
    latent_pre = jnp.dot(normed, pieces[2], preferred_element_type=jnp.float32)
    rope_pre = jnp.dot(normed, pieces[3], preferred_element_type=jnp.float32)
    gated_rows = (value_pre * jax.nn.sigmoid(gate_pre)).astype(jnp.bfloat16)
    conv_reach = conv_taps.shape[0] - 1
    prior_rows = passed_along(gated_rows[row_count - conv_reach :], "sp", 1)
    padded = jnp.concatenate([prior_rows, gated_rows], axis=0).astype(jnp.float32)
    mixed = jnp.zeros(gated_rows.shape, jnp.float32)
    for tap_index in range(conv_taps.shape[0]):
        mixed = (
            mixed
            + conv_taps[tap_index].astype(jnp.float32) * padded[tap_index : tap_index + row_count]
        )
    channel_total = mixed.shape[1] * tp_count
    stat_sum, stat_squares = packed_total(
        (jnp.sum(mixed, axis=1), jnp.sum(mixed * mixed, axis=1)), TP
    )
    channel_mean = stat_sum / channel_total
    channel_var = stat_squares / channel_total - channel_mean * channel_mean
    conv_out = jax.nn.silu(
        (mixed - channel_mean[:, None]) * lax.rsqrt(channel_var + epsilon)[:, None] * conv_gain
    ).astype(jnp.bfloat16)
    head_count = key_up_weight.shape[1] // PLAIN_QK_WIDTH
    latent_width = latent_down_weight.shape[1]
    query = (
        jnp.dot(normed, w_query, preferred_element_type=jnp.float32)
        .astype(jnp.bfloat16)
        .reshape(row_count, head_count, PLAIN_QK_WIDTH + QK_ROPE)
    )
    query_angles = angles_at(query_index.astype(jnp.float32), QK_ROPE)
    query_rope = rotate(
        query[..., PLAIN_QK_WIDTH:].astype(jnp.float32), query_angles[:, None, :]
    ).astype(jnp.bfloat16)
    key_expanded = key_up_weight.reshape(latent_width, head_count, PLAIN_QK_WIDTH)
    query_latent = jnp.einsum(
        "thd,lhd->thl",
        query[..., :PLAIN_QK_WIDTH],
        key_expanded,
        preferred_element_type=jnp.float32,
    ).astype(jnp.bfloat16)
    latent = (
        latent_pre
        * lax.rsqrt(jnp.mean(latent_pre * latent_pre, axis=-1, keepdims=True) + epsilon)
        * latent_norm_gain
    ).astype(jnp.bfloat16)
    key_rope = rotate(rope_pre, angles_at(query_index.astype(jnp.float32), QK_ROPE)).astype(
        jnp.bfloat16
    )
    score_scale = (PLAIN_QK_WIDTH + QK_ROPE) ** (-0.5)
    running_max = jnp.full((row_count, head_count), masked_score, jnp.float32)
    latent_piece, rope_piece = side_by_side((latent, key_rope), "sp", 0, 1)
    piece_rows = latent_piece.shape[0]
    scores = jnp.einsum(
        "thl,kl->thk", query_latent, latent_piece, preferred_element_type=jnp.float32
    )
    scores = (
        scores
        + jnp.einsum("thr,kr->thk", query_rope, rope_piece, preferred_element_type=jnp.float32)
    ) * score_scale
    piece_index = jnp.arange(piece_rows, dtype=jnp.int32)
    allowed = piece_index[None, None, :] <= query_index[:, None, None]
    scores = jnp.where(allowed, scores, masked_score)
    new_max = jnp.maximum(running_max, jnp.max(scores, axis=-1))
    weights = jnp.where(allowed, jnp.exp(scores - new_max[..., None]), 0.0)
    running_sum = jnp.sum(weights, axis=-1)
    weighted = jnp.einsum(
        "thk,kl->thl",
        weights.astype(jnp.bfloat16),
        latent_piece,
        preferred_element_type=jnp.float32,
    )
    running_max, running_sum, weighted = (new_max, running_sum, weighted)
    latent_result = (weighted / running_sum[..., None]).astype(jnp.bfloat16)
    log_sums = running_max + jnp.log(running_sum)
    value_expanded = value_up_weight.reshape(latent_width, head_count, VALUE_HEAD_WIDTH)
    attention = (
        jnp.einsum(
            "thl,lhv->thv", latent_result, value_expanded, preferred_element_type=jnp.float32
        )
        .astype(jnp.bfloat16)
        .reshape(row_count, head_count * VALUE_HEAD_WIDTH)
    )
    merged = summed_on_arrival(
        (
            jnp.dot(conv_out, w_merge_conv, preferred_element_type=jnp.float32)
            + jnp.dot(attention, w_merge_attn, preferred_element_type=jnp.float32)
        ).astype(jnp.bfloat16),
        TP,
        0,
    )
    return (merged.astype(jnp.bfloat16), log_sums)


def solution(mesh):
    finer = Mesh(mesh.devices.reshape(mesh.shape["sp"], 4, 2), ("sp", "tp_0", "tp_1"))
    return jax.shard_map(
        local,
        mesh=finer,
        in_specs=(
            P("sp", TP),
            P(),
            P("sp", TP),
            P("sp", TP),
            P(None, TP),
            P(TP),
            P(None, TP),
            P("sp", None),
            P(),
            P("sp", None),
            P(None, TP),
            P(None, TP),
            P(TP, None),
            P(TP, None),
        ),
        out_specs=(P(SP_TP, None), P("sp", TP)),
        check_vma=False,
    )
```

profile of v0, /device:TPU:1, one launch (start us, length us, event | category | flops | bytes accessed | tf_op | source)
XLA Modules:
  0.0 379.7 jit_solution(15757890945075263962)
XLA Ops:
  7.2 0.0 all-gather.5.cloned.1.call-start
  7.2 1.5 pad_maximum_fusion.2
  8.8 0.0 all-gather.5.cloned.1.call-update
  8.8 0.0 all-gather.7.cloned.1.call-start
  8.8 0.8 fusion.87
  9.6 10.3 %all-gather = bf16[256,256]{1,0:T(8,128)(2,1)S(1)} all-gather(bf16[64,256]{1,0:T(8,128)(2,1)S(1)} %get-tuple-element.7), channel_id=2, replica_groups=mesh['sp'=64,'tp_0'=4,'tp_1'=2] {'tp_0'}, dimensions={0}, use_global_device_ids=true | all-gather | bytes 163840 | tf_op jit(solution)/shard_map/all_gather | solution.py:29
  19.9 10.2 %all_gather.19 = bf16[8,64,256]{2,1,0:T(8,128)(2,1)S(1)} all-gather(bf16[4,64,256]{2,1,0:T(8,128)(2,1)S(1)} %bitcast.92), channel_id=1, replica_groups=mesh['sp'=64,'tp_0'=4,'tp_1'=2] {'tp_1'}, dimensions={0}, use_global_device_ids=true | all-gather | bytes 393216 | tf_op jit(solution)/shard_map/all_gather | solution.py:29
  30.1 1.9 all-gather.1
  31.9 9.4 %all_gather.21 = bf16[8,64,256]{2,1,0:T(8,128)(2,1)S(1)} all-gather(bf16[2,64,256]{2,1,0:T(8,128)(2,1)S(1)} %bitcast.95), channel_id=1, replica_groups=mesh['sp'=64,'tp_0'=4,'tp_1'=2] {'tp_0'}, dimensions={0}, use_global_device_ids=true | all-gather | bytes 327680 | tf_op jit(solution)/shard_map/all_gather | solution.py:29
  41.3 1.1 convert_bitcast_fusion
  42.4 1.5 copy.87
  43.9 0.2 fusion.27
  44.2 1.0 fusion.32
  45.2 109.4 %all-gather.5.cloned.1.call-done = bf16[2048,1088]{1,0:T(8,128)(2,1)} async-done(((bf16[32,1088]{1,0:T(8,128)(2,1)}), bf16[2048,1088]{1,0:T(8,128)(2,1)}) %all-gather.5.cloned.1.call-update) | async-done | bytes 4456464 | tf_op jit(solution)/shard_map/all_gather | solution.py:56
  154.6 1.4 fusion.33
  156.0 0.1 multiply_cosine_fusion
  156.1 0.1 copy.93
  156.2 0.1 copy.92
  156.4 2.2 multiply_reduce_fusion
  158.6 0.1 multiply_convert_fusion
  158.7 0.8 pad_maximum_fusion.1
  159.4 0.5 convolution_convert_fusion.1
  159.9 0.1 copy.89
  160.1 0.7 slice_convert_fusion.31
  160.7 0.6 slice_convert_fusion
  161.4 0.7 iota_compare_fusion
  162.0 1.6 fusion.29
  163.6 1.6 fusion.18
  165.3 1.3 collective-permute-start
  166.6 1.1 copy.98
  167.7 0.9 maximum_convert_fusion
  168.6 1.3 fusion.85
  170.0 0.6 broadcast_in_dim.24
  170.6 14.6 %all-to-all-start = ((f32[8,1,256]{2,1,0:T(1,128)}), f32[8,1,256]{2,1,0:T(1,128)S(1)}, u32[]{:S(2)}, u32[]{:S(2)}) async-start(f32[8,1,256]{2,1,0:T(1,128)} %broadcast_in_dim.24), calls=%async_computation | async-start | bytes 16384 | tf_op jit(solution)/shard_map/all_to_all | solution.py:71
  185.2 0.8 subtract_convert_fusion
  186.0 3.8 %all-to-all-done = f32[8,1,256]{2,1,0:T(1,128)S(1)} async-done(((f32[8,1,256]{2,1,0:T(1,128)}), f32[8,1,256]{2,1,0:T(1,128)S(1)}, u32[]{:S(2)}, u32[]{:S(2)}) %all-to-all-start) | async-done | bytes 8224 | tf_op jit(solution)/shard_map/all_to_all | solution.py:71
  189.8 2.6 fusion.70
  192.5 126.7 %all-gather.7.cloned.1.call-done = bf16[8192,576]{1,0:T(8,128)(2,1)} async-done(((bf16[128,576]{1,0:T(8,128)(2,1)}), bf16[8192,576]{1,0:T(8,128)(2,1)}) %all-gather.7.cloned.1.call-update) | async-done | bytes 9437200 | tf_op jit(solution)/shard_map/all_gather | solution.py:56
  319.1 9.2 %fusion.5 = f32[128,2,8192]{2,0,1:T(8,128)} fusion(bf16[8192,576]{1,0:T(8,128)(2,1)} %all-gather.7.cloned.1.call-done, bf16[128,2,192]{0,2,1:T(8,128)(2,1)S(1)} %bitcast.94, bf16[512,256]{1,0:T(8,128)(2,1)S(1)} %copy-done.2), kind=kOutput, calls=%fused_computation.8 | convolution fusion | flops 2181169152 | bytes 17104896 | tf_op jit(solution)/shard_map/thl,kl->thk/dot_general | solution.py:193
  328.3 6.5 %fusion.88 = (f32[128,2]{0,1:T(2,128)S(1)}, f32[128,2,8192]{2,0,1:T(8,128)S(1)}) fusion(f32[128,2,8192]{2,0,1:T(8,128)} %fusion.5, bf16[8192,576]{1,0:T(8,128)(2,1)} %all-gather.7.cloned.1.call-done, bf16[128,2,32]{0,2,1:T(8,128)(2,1)S(1)} %get-tuple-element.6, bf16[128,2,32]{0,2,1:T(8,128)(2,1)S(1)} %get-tuple-element.5, ...), kind=kOutput, calls=%fused_computation.175 | convolution fusion | flops 276889344 | bytes 19956736 | tf_op jit(solution)/shard_map/thr,kr->thk/dot_general | solution.py:198
  334.8 3.3 copy-done.1
  338.1 2.1 fusion.2
  340.3 8.4 %convolution_convert_fusion.2 = bf16[2,128,128]{1,2,0:T(8,128)(2,1)S(1)} fusion(bf16[512,2,128]{0,2,1:T(8,128)(2,1)S(1)} %bitcast.96, bf16[8192,576]{1,0:T(8,128)(2,1)} %all-gather.7.cloned.1.call-done, f32[128,2,8192]{2,0,1:T(8,128)} %copy-done.1, f32[128,2]{0,1:T(2,128)S(1)} %broadcast_maximum_fusion, pred[128,8192]{1,0:T(8,128)(4,1)S(1)} %iota_compare_fusion, ...), kind=kOutput, calls=%fused_computation.29 | convolution fusion | flops 2187624448 | bytes 18155520 | tf_op jit(solution)/shard_map/thl,lhv->thv/dot_general | solution.py:217
  348.6 2.7 fusion.10
  351.3 11.5 %all-to-all-start.1 = ((bf16[8,16,2048]{2,1,0:T(8,128)(2,1)}), bf16[8,16,2048]{2,1,0:T(8,128)(2,1)S(1)}, u32[]{:S(2)}, u32[]{:S(2)}) async-start(bf16[8,16,2048]{2,1,0:T(8,128)(2,1)} %bitcast.45), calls=%async_computation.1 | async-start | bytes 1048576 | tf_op jit(solution)/shard_map/all_to_all | solution.py:94
  362.8 0.6 log_add_fusion
  363.4 8.8 %all-to-all-done.1 = bf16[8,16,2048]{2,1,0:T(8,128)(2,1)S(1)} async-done(((bf16[8,16,2048]{2,1,0:T(8,128)(2,1)}), bf16[8,16,2048]{2,1,0:T(8,128)(2,1)S(1)}, u32[]{:S(2)}, u32[]{:S(2)}) %all-to-all-start.1) | async-done | bytes 524320 | tf_op jit(solution)/shard_map/all_to_all | solution.py:94
  372.2 0.7 reduce_sum.72
  (25 shorter events, 0.2 us)
Async XLA Ops:
  7.2 152.3 %copy-start = (bf16[2048,384]{1,0:T(8,128)(2,1)S(1)}, bf16[2048,384]{1,0:T(8,128)(2,1)}, u32[]{:S(2)}) copy-start(bf16[2048,384]{1,0:T(8,128)(2,1)} %param.20) | copy-start | bytes 4718596
  7.2 151.4 %copy-start.5 = (f32[512]{0:T(512)S(1)}, f32[512]{0:T(512)}, u32[]{:S(2)}) copy-start(f32[512]{0:T(512)} %param.22) | copy-start | bytes 6148
  7.2 152.9 %copy-start.4 = (bf16[31,256]{1,0:T(8,128)(2,1)S(1)}, bf16[31,256]{1,0:T(8,128)(2,1)}, u32[]{:S(2)}) copy-start(bf16[31,256]{1,0:T(8,128)(2,1)} %param.18) | copy-start | bytes 47620
  7.2 147.4 %all-gather.5.cloned.1.call-start = ((), (), s32[]{:S(2)}) async-start(), calls=%async_computation.2 | async-start | bytes 4792320 | tf_op jit(solution)/shard_map/all_gather | solution.py:56
  8.8 310.3 %all-gather.7.cloned.1.call-start = ((), (), s32[]{:S(2)}) async-start(), calls=%async_computation.3 | async-start | bytes 10649600 | tf_op jit(solution)/shard_map/all_gather | solution.py:56
  158.5 160.6 %copy-start.2 = (bf16[512,256]{1,0:T(8,128)(2,1)S(1)}, bf16[512,256]{1,0:T(8,128)(2,1)}, u32[]{:S(2)}) copy-start(bf16[512,256]{1,0:T(8,128)(2,1)} %param.24) | copy-start | bytes 786436
  165.2 1.3 copy-start.3
  165.3 2.4 collective-permute-start
  170.6 19.2 %all-to-all-start = ((f32[8,1,256]{2,1,0:T(1,128)}), f32[8,1,256]{2,1,0:T(1,128)S(1)}, u32[]{:S(2)}, u32[]{:S(2)}) async-start(f32[8,1,256]{2,1,0:T(1,128)} %broadcast_in_dim.24), calls=%async_computation | async-start | bytes 16384 | tf_op jit(solution)/shard_map/all_to_all | solution.py:71
  334.8 3.3 copy-start.1
  351.3 20.9 %all-to-all-start.1 = ((bf16[8,16,2048]{2,1,0:T(8,128)(2,1)}), bf16[8,16,2048]{2,1,0:T(8,128)(2,1)S(1)}, u32[]{:S(2)}, u32[]{:S(2)}) async-start(bf16[8,16,2048]{2,1,0:T(8,128)(2,1)} %bitcast.45), calls=%async_computation.1 | async-start | bytes 1048576 | tf_op jit(solution)/shard_map/all_to_all | solution.py:94
Sparse Core Ops, SparseCore 0:
  11.0 143.6 all-gather.4
  159.6 159.5 all-gather.6
where the time goes:
time: 381 us; the launch traced here: 380 us
  waiting for transfers between devices  249 us (65%)
  matrix products  36.5 us (10%)
  blocking collectives  31.7 us (8%)
  starting transfers between devices  27.5 us (7%)
  between operations  14.3 us (4%)
  other arithmetic  13.3 us (3%)
  local copies, waits for them, and re-layouts  7.75 us (2%)
    all_gather x2, waiting for transfers between devices, side_by_side(): result, at, done = (lax.all_gather(both, axis, axis=dim, tiled=True), 0, [])  236 us
    all_gather x4, blocking collectives, all_blocks(): parts = lax.all_gather(parts, axes[k], axis=0, tiled=True)  31.7 us
    all_to_all x1, starting transfers between devices, sent_to_all(): return lax.all_to_all(copies, axis, split_axis=0, concat_axis=0, tiled=True)  14.6 us
    all_to_all x1, starting transfers between devices, summed_on_arrival(): parts = lax.all_to_all(split_up(shard, dim, count), axis, 0, 0, tiled=True)  11.5 us
    dot_general x1, matrix products, local(): jnp.einsum('thl,kl->thk', query_latent, latent_piece, preferred_element_t...  9.22 us
    all_to_all x1, waiting for transfers between devices, summed_on_arrival(): parts = lax.all_to_all(split_up(shard, dim, count), axis, 0, 0, tiled=True)  8.78 us
    dot_general x1, matrix products, local(): jnp.einsum('thl,lhv->thv', latent_result, value_expanded, preferred_eleme...  8.36 us
  transfers between devices with their start and end apart: 5, of which 4 were waited for; matrix products, arithmetic and copies ran while one was open for 5% of the time, Pallas kernels for 0%

commit v1 on v0

v1 whole, which is shorter than its diff:
```python
import functools

import jax
import jax.numpy as jnp
from jax import lax
from jax.experimental import pallas as pl
from jax.experimental.pallas import tpu as pltpu
from jax.sharding import Mesh
from jax.sharding import PartitionSpec as P

PLAIN_QK_WIDTH = 128
QK_ROPE = 64
VALUE_HEAD_WIDTH = 128
epsilon = 1e-06
rope_base = 10000.0
masked_score = -1e30
SP = ("z", "y")
TP = ("x", "c")
LANES = 128
VMEM = pl.BlockSpec(memory_space=pltpu.VMEM)
MIB = 1 << 20


class Net:
    def __init__(self, sizes, send, recv):
        self.nz, self.ny, self.nx, self.nc = sizes
        self.z, self.y, self.x, self.c = (lax.axis_index(a) for a in ("z", "y", "x", "c"))
        self.send, self.recv = send, recv
        self.ids, self.open = {}, []

    def number(self, name):
        return self.ids.setdefault(name, len(self.ids))

    def put(self, name, src, dst, **to):
        k = self.number(name)
        copy = pltpu.make_async_remote_copy(
            src_ref=src,
            dst_ref=dst,
            send_sem=self.send.at[k],
            recv_sem=self.recv.at[k],
            device_id=to,
            device_id_type=pl.DeviceIdType.MESH,
        )
        copy.start()
        self.open.append(copy)

    def got(self, name, dst, **to):
        k = self.number(name)
        pltpu.make_async_remote_copy(
            src_ref=dst,
            dst_ref=dst,
            send_sem=self.send.at[k],
            recv_sem=self.recv.at[k],
            device_id=to,
            device_id_type=pl.DeviceIdType.MESH,
        ).wait_recv()

    def finish(self):
        for copy in self.open:
            copy.wait_send()

    def zp(self, d):
        return lax.rem(self.z + d + self.nz, self.nz)

    def yp(self, d):
        return lax.rem(self.y + d + self.ny, self.ny)

    def xp(self, d):
        return lax.rem(self.x + d + self.nx, self.nx)

    def cp(self):
        return 1 - self.c

    def greet(self, peers):
        barrier = pltpu.get_barrier_semaphore()
        for to in peers:
            pl.semaphore_signal(barrier, inc=1, device_id=to, device_id_type=pl.DeviceIdType.MESH)
        pl.semaphore_wait(barrier, len(peers))


def z_plan(nz):
    group = 4 if nz >= 16 else 2
    count = nz // group
    if group == 4:
        near = {1: range(count), -1: range(count), 2: (0, 1), -2: (1, 2)}
    else:
        near = {1: range(count)}
    return group, count, near


def z_peers(net):
    group, count, near = z_plan(net.nz)
    far = (1, -1) if count > 2 else (1,) if count == 2 else ()
    offsets = [group * f for f in far]
    for d in near:
        offsets.append(d)
    peers = [{"z": net.zp(d)} for d in offsets]
    if group == 2:
        peers.append({"z": net.zp(-1)})
    return peers


class ZGather:
    def __init__(self, net, tag, slot):
        self.net, self.tag, self.slot = net, tag, slot
        self.group, self.count, self.near = z_plan(net.nz)
        z_class = net.z // self.group
        self.turn = jnp.where(lax.rem(z_class, 2) == 1, 1, -1)

    def block(self, b):
        return self.slot(self.net.zp(b * self.group))

    def start(self):
        n, g = self.net, self.group
        own = self.block(0)
        if self.count >= 2:
            n.put((self.tag, "f", 1), own, own, z=n.zp(g))
        if self.count > 2:
            n.put((self.tag, "f", -1), own, own, z=n.zp(-g))
        self.spread(0)

    def spread(self, b):
        n = self.net
        for d, blocks in self.near.items():
            if b in blocks:
                n.put((self.tag, "n", d, b), self.block(b), self.block(b), z=n.zp(d))

    def far(self):
        n, g = self.net, self.group
        if self.count == 2:
            n.got((self.tag, "f", 1), self.block(1), z=n.zp(g))
            self.spread(1)
            yield g
            return
        n.got((self.tag, "f", 1), self.block(3), z=n.zp(g))
        n.got((self.tag, "f", -1), self.block(1), z=n.zp(g))
        onward = self.slot(n.zp(-g * self.turn))
        n.put((self.tag, "r"), onward, onward, z=n.zp(g * self.turn))
        self.spread(1)
        self.spread(3)
        yield g
        yield 3 * g
        n.got((self.tag, "r"), self.block(2), z=n.zp(g))
        self.spread(2)
        yield 2 * g

    def close(self):
        n, g = self.net, self.group
        order = (0, 1, 3, 2) if self.count == 4 else range(self.count)
        for b in order:
            for d, blocks in self.near.items():
                if b in blocks:
                    at = (b * g - d) % n.nz
                    n.got((self.tag, "n", d, b), self.slot(n.zp(at)), z=n.zp(d))
                    yield at


def tile(i, size):
    return pl.ds(pl.multiple_of(i * size, size), size)


def gather_inputs(sizes, tok, lw, vg, X, WL, VG, yb, send, recv):
    net = Net(sizes, send, recv)
    nz, ny, nx, nc = sizes
    z, y, x, c = net.z, net.y, net.x, net.c
    half = tok.shape[1] // 2
    wr = lw.shape[0]
    kept = WL.shape[0]

    peers = [{"y": net.yp(k)} for k in range(1, ny)] + [{"x": net.xp(k)} for k in range(1, nx)]
    peers += [{"c": net.cp()}] + z_peers(net)
    net.greet(peers)

    def cols(side, xx, cc):
        return tile((xx * nc + cc) * 2 + side, half)

    def place(side, yy, xx, cc):
        return X.at[yy, :, cols(side, xx, cc)]

    mine = [tok.at[:, pl.ds(0, half)], tok.at[:, pl.ds(half, half)]]
    for k in range(1, ny):
        net.put(("lw", k), lw, yb.at[y], y=net.yp(k))
    for k in range(1, ny):
        net.put(("ya", k), mine[0], place(0, y, x, c), y=net.yp(k))
    for k in range(1, nx):
        net.put(("xb", k), mine[1], place(1, y, x, c), x=net.xp(k))
    for k in range(1, nx):
        net.put(("xa", 0, k), mine[0], place(0, y, x, c), x=net.xp(k))
    for k in range(1, ny):
        net.put(("yb", 0, k), mine[1], place(1, y, x, c), y=net.yp(k))
    for k in range(1, ny):
        net.put(("vg", k), vg.at[net.yp(k)], VG.at[tile(y, wr)], y=net.yp(k))
    for side in (0, 1):
        net.put(("s", side), mine[side], place(side, y, x, c), c=net.cp())
        X[pl.ds(y, 1), :, cols(side, x, c)] = tok[:, side * half : (side + 1) * half][None]
    yb[pl.ds(y, 1)] = lw[...][None]
    VG[tile(y, wr)] = vg[pl.ds(y, 1)].reshape(vg.shape[1:])

    for k in range(1, ny):
        net.got(("lw", k), yb.at[net.yp(-k)], y=net.yp(k))
    rows = yb[...].reshape(ny * wr, yb.shape[2])
    WL[:, tile(z, LANES)] = rows.astype(jnp.float32).T[:kept].astype(WL.dtype)
    zg = ZGather(net, "wl", lambda at: WL.at[:, tile(at, LANES)])
    zg.start()

    for k in range(1, ny):
        here = place(0, net.yp(-k), x, c)
        net.got(("ya", k), here, y=net.yp(k))
        for j in range(1, nx):
            net.put(("xa", k, j), here, here, x=net.xp(j))
        net.put(("sa", k), here, here, c=net.cp())
    for k in range(1, nx):
        here = place(1, y, net.xp(-k), c)
        net.got(("xb", k), here, x=net.xp(k))
        for j in range(1, ny):
            net.put(("yb", k, j), here, here, y=net.yp(j))
        net.put(("sb", k), here, here, c=net.cp())
    for _ in zg.far():
        pass
    for k in range(ny):
        for j in range(1, nx):
            here = place(0, net.yp(-k), net.xp(-j), c)
            net.got(("xa", k, j), here, x=net.xp(j))
            net.put(("sxa", k, j), here, here, c=net.cp())
    for k in range(nx):
        for j in range(1, ny):
            here = place(1, net.yp(-j), net.xp(-k), c)
            net.got(("yb", k, j), here, y=net.yp(j))
            net.put(("syb", k, j), here, here, c=net.cp())
    for _ in zg.close():
        pass
    for k in range(1, ny):
        net.got(("vg", k), VG.at[tile(net.yp(-k), wr)], y=net.yp(k))
    o = net.cp()
    for side in (0, 1):
        net.got(("s", side), place(side, y, x, o), c=o)
    for k in range(1, ny):
        net.got(("sa", k), place(0, net.yp(-k), x, o), c=o)
    for k in range(1, nx):
        net.got(("sb", k), place(1, y, net.xp(-k), o), c=o)
    for k in range(ny):
        for j in range(1, nx):
            net.got(("sxa", k, j), place(0, net.yp(-k), net.xp(-j), o), c=o)
    for k in range(nx):
        for j in range(1, ny):
            net.got(("syb", k, j), place(1, net.yp(-j), net.xp(-k), o), c=o)
    net.finish()


def gather_latent(sizes, own, vg, K, W, send, recv):
    net = Net(sizes, send, recv)
    nz, ny, nx, nc = sizes
    z, x, c = net.z, net.x, net.c
    depth = vg.shape[0]

    peers = [{"x": net.xp(k)} for k in range(1, nx)] + [{"c": net.cp()}] + z_peers(net)
    net.greet(peers)

    def slot(at, xx=None, cc=None):
        j = (x if xx is None else xx) * nc + (c if cc is None else cc)
        return K.at[j, :, tile(at, own.shape[1])]

    K[pl.ds(x * nc + c, 1), :, tile(z, own.shape[1])] = own[...][None]
    W[tile(z, depth)] = vg[...]
    zl = ZGather(net, "l", slot)
    zw = ZGather(net, "w", lambda at: W.at[tile(at, depth)])

    def onward(n):
        here = slot(net.zp(n))
        for k in range(1, nx):
            net.put(("x", n, k), here, here, x=net.xp(k))
        net.put(("s", n), here, here, c=net.cp())

    zl.start()
    onward(0)
    zw.start()
    for n in zl.far():
        onward(n)
    for _ in zw.far():
        pass
    order = [0] + [zl.group * b for b in ((1, 3, 2) if zl.count == 4 else range(1, zl.count))]
    for n in zl.close():
        onward(n)
        order.append(n)
    for n in order:
        for k in range(1, nx):
            here = slot(net.zp(n), net.xp(-k))
            net.got(("x", n, k), here, x=net.xp(k))
            net.put(("sx", n, k), here, here, c=net.cp())
    for _ in zw.close():
        pass
    o = net.cp()
    for n in order:
        net.got(("s", n), slot(net.zp(n), None, o), c=o)
        for k in range(1, nx):
            net.got(("sx", n, k), slot(net.zp(n), net.xp(-k), o), c=o)
    net.finish()


def exchange(sizes, att, mixed, st, att_r, mixed_r, st_r, stat_r, send, recv):
    net = Net(sizes, send, recv)
    nz, ny, nx, nc = sizes
    y, x, c = net.y, net.x, net.c
    rows = att_r.shape[2]
    offsets = [(a, b) for a in range(nx) for b in range(nc) if a or b]

    def there(a, b):
        return {"x": net.xp(a), "c": net.c if b == 0 else net.cp()}

    net.greet([{"y": net.yp(k)} for k in range(1, ny)] + [there(a, b) for a, b in offsets])
    for k in range(1, ny):
        t = net.yp(k)
        net.put(("st", k), st.at[t], st_r.at[y], y=t)
    for k in range(1, ny):
        t = net.yp(k)
        net.put(("m", k), mixed.at[t], mixed_r.at[y], y=t)
        net.put(("a", k), att.at[:, tile(t, rows), :], att_r.at[y], y=t)
    att_r[pl.ds(y, 1)] = att[:, tile(y, rows), :][None]
    mixed_r[pl.ds(y, 1)] = mixed[pl.ds(y, 1)]
    st_r[pl.ds(y, 1)] = st[pl.ds(y, 1)]
    for k in range(1, ny):
        net.got(("st", k), st_r.at[net.yp(-k)], y=net.yp(k))
    me = x * nc + c
    stat_r[pl.ds(me, 1)] = jnp.sum(st_r[...], axis=0)[None]
    for a, b in offsets:
        net.put(("t", a, b), stat_r.at[me], stat_r.at[me], **there(a, b))
    for k in range(1, ny):
        net.got(("m", k), mixed_r.at[net.yp(-k)], y=net.yp(k))
        net.got(("a", k), att_r.at[net.yp(-k)], y=net.yp(k))
    for a, b in offsets:
        j = net.xp(-a) * nc + (net.c if b == 0 else net.cp())
        net.got(("t", a, b), stat_r.at[j], **there(a, b))
    net.finish()


def scatter_rows(sizes, part, out, send, recv):
    net = Net(sizes, send, recv)
    nz, ny, nx, nc = sizes
    x, c = net.x, net.c
    me = x * nc + c
    offsets = [(a, b) for a in range(nx) for b in range(nc) if a or b]

    def there(a, b):
        return {"x": net.xp(a), "c": net.c if b == 0 else net.cp()}

    def index(to):
        return to["x"] * nc + to["c"]

    net.greet([there(a, b) for a, b in offsets])
    for a, b in offsets:
        to = there(a, b)
        net.put((a, b), part.at[index(to)], out.at[me], **to)
    out[pl.ds(me, 1)] = part[pl.ds(me, 1)]
    for a, b in offsets:
        source = there(-a, b)
        net.got((a, b), out.at[index(source)], **there(a, b))
    net.finish()


def kernel_call(body, sizes, outs, messages, cid, args, scratch=(), limit=24 * MIB):
    return pl.pallas_call(
        functools.partial(body, sizes),
        out_shape=outs,
        in_specs=[VMEM] * len(args),
        out_specs=[VMEM] * len(outs),
        scratch_shapes=[
            *scratch,
            pltpu.SemaphoreType.DMA((messages,)),
            pltpu.SemaphoreType.DMA((messages,)),
        ],
        compiler_params=pltpu.CompilerParams(
            collective_id=cid, has_side_effects=True, vmem_limit_bytes=limit
        ),
        name=body.__name__,
    )(*args)


def attend(blocks, scale, ql, qr, lat, rope, up, att, ml):
    i = pl.program_id(0)
    rows = ql.shape[0]
    keys = lat.shape[1]
    plane = blocks * rows
    s = jnp.dot(ql[...], lat[...], preferred_element_type=jnp.float32)
    s = s + jnp.dot(qr[...], rope[...], preferred_element_type=jnp.float32)
    z, y = lax.axis_index("z"), lax.axis_index("y")
    ny = lax.axis_size("y")
    per = plane // ny
    query_at = z * plane + lax.rem(i, blocks) * rows + lax.broadcasted_iota(jnp.int32, (rows, 1), 0)
    lane = lax.broadcasted_iota(jnp.int32, (1, keys), 1)
    key_at = (lane // per) * plane + y * per + lax.rem(lane, per)
    allowed = key_at <= query_at
    s = jnp.where(allowed, s * scale, masked_score)
    top = jnp.max(s, axis=1, keepdims=True)
    w = jnp.where(allowed, jnp.exp(s - top), 0.0)
    total = jnp.sum(w, axis=1, keepdims=True)
    mixed = lax.dot_general(
        w.astype(jnp.bfloat16), lat[...], (((1,), (1,)), ((), ())), preferred_element_type=jnp.float32
    )
    share = (mixed / jnp.maximum(total, 1e-30)).astype(jnp.bfloat16)
    att[...] = jnp.dot(share, up[...], preferred_element_type=jnp.float32).astype(jnp.bfloat16)
    side = lax.broadcasted_iota(jnp.int32, (rows, LANES), 1)
    ml[...] = jnp.where(side == 0, top, total).T[:8]


def attention_call(ql, qr, lat, rope, up, heads, plane):
    rows = min(256, plane)
    blocks = plane // rows
    scale = (PLAIN_QK_WIDTH + QK_ROPE) ** (-0.5)
    total, width = ql.shape
    v = up.shape[1] // heads
    flops = 2 * total * lat.shape[1] * (2 * width + qr.shape[1]) + 2 * total * width * v
    return pl.pallas_call(
        functools.partial(attend, blocks, scale),
        grid=(total // rows,),
        out_shape=[
            jax.ShapeDtypeStruct((total, v), jnp.bfloat16),
            jax.ShapeDtypeStruct((8, total), jnp.float32),
        ],
        in_specs=[
            pl.BlockSpec((rows, width), lambda i: (i, 0)),
            pl.BlockSpec((rows, qr.shape[1]), lambda i: (i, 0)),
            pl.BlockSpec(lat.shape, lambda i: (0, 0)),
            pl.BlockSpec(rope.shape, lambda i: (0, 0)),
            pl.BlockSpec((width, v), lambda i: (0, i // blocks)),
        ],
        out_specs=[
            pl.BlockSpec((rows, v), lambda i: (i, 0)),
            pl.BlockSpec((8, rows), lambda i: (0, i)),
        ],
        compiler_params=pltpu.CompilerParams(vmem_limit_bytes=32 * MIB),
        cost_estimate=pl.CostEstimate(
            flops=flops, bytes_accessed=6 * MIB, transcendentals=total * lat.shape[1]
        ),
        name="attend",
    )(ql, qr, lat, rope, up)


def angles_at(positions, indices, width):
    inverse = rope_base ** (-2.0 * indices.astype(jnp.float32) / width)
    return positions[:, None] * inverse[None, :]


def local(
    tokens,
    norm_gain,
    w_value,
    w_gate,
    conv_taps,
    conv_gain,
    w_query,
    latent_down_weight,
    latent_norm_gain,
    w_rope_key,
    key_up_weight,
    value_up_weight,
    w_merge_conv,
    w_merge_attn,
):
    bf16, f32 = jnp.bfloat16, jnp.float32
    sizes = nz, ny, nx, nc = tuple(lax.axis_size(a) for a in ("z", "y", "x", "c"))
    z, y, x, c = (lax.axis_index(a) for a in ("z", "y", "x", "c"))
    ntp = nx * nc
    j = x * nc + c
    rows, feats = tokens.shape
    width = feats * ntp
    plane = rows * ny
    wr, chans = w_value.shape
    share = chans // ny
    rank = latent_down_weight.shape[1]
    lat_share, rope_share = rank // ntp, QK_ROPE // ntp
    pairs = rope_share // 2
    kept = lat_share + rope_share
    middle = QK_ROPE // 2

    rope_cols = w_rope_key.reshape(wr, 2, ntp, pairs)
    rope_part = lax.dynamic_slice_in_dim(rope_cols, j, 1, 2).reshape(wr, rope_share)
    lat_part = lax.dynamic_slice_in_dim(latent_down_weight, j * lat_share, lat_share, 1)
    lw = jnp.concatenate([lat_part, rope_part, jnp.zeros((wr, LANES - kept), bf16)], axis=1)
    vg = jnp.concatenate(
        [w_value.reshape(wr, ny, share), w_gate.reshape(wr, ny, share)], axis=2
    ).transpose(1, 0, 2)

    messages = (3 + 2 * ny + 3 * nx) + 2 * ny + 4 * nx * ny + 20 + ny + nx
    X, WL, VG = kernel_call(
        gather_inputs,
        sizes,
        [
            jax.ShapeDtypeStruct((ny, rows, width), bf16),
            jax.ShapeDtypeStruct((kept, nz * LANES), bf16),
            jax.ShapeDtypeStruct((ny * wr, 2 * share), bf16),
        ],
        messages,
        0,
        (tokens, lw, vg),
        scratch=[pltpu.VMEM((ny, wr, LANES), bf16)],
    )
    features = X.reshape(plane, width).astype(f32)
    normed = (
        features
        * lax.rsqrt(jnp.mean(features * features, axis=-1, keepdims=True) + epsilon)
        * norm_gain
    ).astype(bf16)
    normed_own = lax.dynamic_slice_in_dim(normed, y * rows, rows, 0)

    pre = lax.dot_general(WL, normed_own, (((1,), (1,)), ((), ())), preferred_element_type=f32)
    first_row = (z * ny + y) * rows
    own_at = (first_row + jnp.arange(rows, dtype=jnp.int32)).astype(f32)
    own_angle = angles_at(own_at, j * pairs + jnp.arange(pairs, dtype=jnp.int32), QK_ROPE).T
    first, second = pre[lat_share : lat_share + pairs], pre[lat_share + pairs :]
    cosine, sine = jnp.cos(own_angle), jnp.sin(own_angle)
    own = jnp.concatenate(
        [pre[:lat_share], first * cosine - second * sine, first * sine + second * cosine], axis=0
    ).astype(bf16)

    K, W = kernel_call(
        gather_latent,
        sizes,
        [
            jax.ShapeDtypeStruct((ntp, kept, nz * rows), bf16),
            jax.ShapeDtypeStruct((nz * ny * wr, 2 * share), bf16),
        ],
        2 * 20 + nz * (2 * nx),
        1,
        (own, VG),
    )
    keys = nz * rows
    raw = K[:, :lat_share].reshape(rank, keys).astype(f32)
    latent = (
        raw
        * lax.rsqrt(jnp.mean(raw * raw, axis=0, keepdims=True) + epsilon)
        * latent_norm_gain[:, None]
    ).astype(bf16)
    key_rope = (
        K[:, lat_share:].reshape(ntp, 2, pairs, keys).transpose(1, 0, 2, 3).reshape(QK_ROPE, keys)
    )

    heads = key_up_weight.shape[1] // PLAIN_QK_WIDTH
    query = (
        jnp.dot(normed, w_query, preferred_element_type=f32)
        .astype(bf16)
        .reshape(plane, heads, PLAIN_QK_WIDTH + QK_ROPE)
    )
    plane_at = (z * plane + jnp.arange(plane, dtype=jnp.int32)).astype(f32)
    angle = angles_at(plane_at, jnp.arange(middle, dtype=jnp.int32), QK_ROPE)[:, None, :]
    turned = query[..., PLAIN_QK_WIDTH:].astype(f32)
    first, second = turned[..., :middle], turned[..., middle:]
    cosine, sine = jnp.cos(angle), jnp.sin(angle)
    query_rope = jnp.concatenate(
        [first * cosine - second * sine, first * sine + second * cosine], axis=-1
    ).astype(bf16)
    query_latent = jnp.einsum(
        "thd,lhd->htl",
        query[..., :PLAIN_QK_WIDTH],
        key_up_weight.reshape(rank, heads, PLAIN_QK_WIDTH),
        preferred_element_type=f32,
    ).astype(bf16)

    both = jnp.dot(normed, W, preferred_element_type=f32)
    gated = (both[:, :share] * jax.nn.sigmoid(both[:, share:])).astype(bf16)
    reach = conv_taps.shape[0] - 1
    prior = lax.ppermute(gated[plane - reach :], "z", [(i, i + 1) for i in range(nz - 1)])

    att, ml = attention_call(
        query_latent.reshape(heads * plane, rank),
        query_rope.transpose(1, 0, 2).reshape(heads * plane, QK_ROPE),
        latent,
        key_rope,
        value_up_weight,
        heads,
        plane,
    )

    taps = lax.dynamic_slice_in_dim(conv_taps, y * share, share, 1).astype(f32)
    padded = jnp.concatenate([prior, gated], axis=0).astype(f32)
    mixed = jnp.zeros(gated.shape, f32)
    for tap in range(reach + 1):
        mixed = mixed + taps[tap] * padded[tap : tap + plane]

    mid = rows // 2
    packed = jnp.concatenate(
        [mixed.reshape(ny, 2, mid, share)[:, 0], mixed.reshape(ny, 2, mid, share)[:, 1]], axis=2
    )
    tops = ml[0].reshape(heads, ny, rows)
    sums = ml[1].reshape(heads, ny, rows)
    stats = jnp.stack([jnp.sum(mixed, axis=1), jnp.sum(mixed * mixed, axis=1)]).reshape(2, ny, rows)
    st = jnp.concatenate([stats, tops, sums], axis=0).transpose(1, 0, 2)
    st = jnp.concatenate([st, jnp.zeros((ny, 8 - st.shape[1], rows), f32)], axis=1)
    att_r, mixed_r, st_r, stat_r = kernel_call(
        exchange,
        sizes,
        [
            jax.ShapeDtypeStruct((ny, heads, rows, VALUE_HEAD_WIDTH), bf16),
            jax.ShapeDtypeStruct((ny, mid, 2 * share), f32),
            jax.ShapeDtypeStruct((ny, 8, rows), f32),
            jax.ShapeDtypeStruct((ntp, 8, rows), f32),
        ],
        3 * ny + ntp,
        2,
        (att.reshape(heads, plane, VALUE_HEAD_WIDTH), packed, st),
    )
    tops, sums = st_r[:, 2 : 2 + heads], st_r[:, 2 + heads : 2 + 2 * heads]
    top = jnp.max(tops, axis=0)
    factor = jnp.exp(tops - top) * sums
    total = jnp.sum(factor, axis=0)
    log_sums = (top + jnp.log(total)).T
    factor = factor / total
    attention = (
        jnp.sum(factor[..., None] * att_r.astype(f32), axis=0)
        .astype(bf16)
        .transpose(1, 0, 2)
        .reshape(rows, heads * VALUE_HEAD_WIDTH)
    )
    channel_stats = jnp.sum(stat_r[:, :2], axis=0)
    channel_total = chans * ntp
    channel_mean = channel_stats[0] / channel_total
    channel_var = channel_stats[1] / channel_total - channel_mean * channel_mean
    own_mixed = (
        mixed_r.reshape(ny, mid, 2, share).transpose(2, 1, 0, 3).reshape(rows, chans)
    )
    conv_out = jax.nn.silu(
        (own_mixed - channel_mean[:, None]) * lax.rsqrt(channel_var + epsilon)[:, None] * conv_gain
    ).astype(bf16)
    part = (
        jnp.dot(conv_out, w_merge_conv, preferred_element_type=f32)
        + jnp.dot(attention, w_merge_attn, preferred_element_type=f32)
    ).astype(bf16)
    (parts,) = kernel_call(
        scatter_rows,
        sizes,
        [jax.ShapeDtypeStruct((ntp, rows // ntp, part.shape[1]), bf16)],
        ntp,
        3,
        (part.reshape(ntp, rows // ntp, part.shape[1]),),
    )
    merged = jnp.sum(parts.astype(f32), axis=0).astype(bf16)
    return merged, log_sums


def solution(mesh):
    devices = mesh.devices
    shape = (devices.shape[0] // 4, 4, 4, 2)
    finer = Mesh(devices.reshape(shape), ("z", "y", "x", "c"))
    return jax.shard_map(
        local,
        mesh=finer,
        in_specs=(
            P(SP, TP),
            P(),
            P(SP, TP),
            P(SP, TP),
            P(None, TP),
            P(TP),
            P(None, TP),
            P(SP, None),
            P(),
            P(SP, None),
            P(None, TP),
            P(None, TP),
            P(TP, None),
            P(TP, None),
        ),
        out_specs=(P((*SP, *TP), None), P(SP, TP)),
        check_vma=False,
    )
```

time: 381 us -> 142 us (0.37)
  waiting for transfers between devices: 249 us -> 0.01 us
  Pallas kernels: 0 us -> 96.9 us
  blocking collectives: 31.7 us -> 0 us
  matrix products: 36.5 us -> 6.67 us
  starting transfers between devices: 27.5 us -> 3.75 us
  between operations: 14.3 us -> 1.46 us
  other arithmetic: 13.3 us -> 20.9 us
  local copies, waits for them, and re-layouts: 7.75 us -> 12 us
    all_gather x2 -> x0, waiting for transfers between devices: 236 us -> none  [side_by_side(): result, at, done = (lax.all_gather(both, axis, axis=dim, tiled=True), 0, [])]
    pallas_call x0 -> x5, Pallas kernels: none -> 96.9 us  [the longest x4 87.9 us: kernel_call(): pl.pallas_call(functools.partial(body, sizes), out_shape=outs, in_specs=[...]
    all_gather x4 -> x0, blocking collectives: 31.7 us -> none  [all_blocks(): parts = lax.all_gather(parts, axes[k], axis=0, tiled=True)]
    dot_general x10 -> x6, matrix products: 36.5 us -> 6.67 us  [the longest x1 2.61 us: local(): jnp.dot(normed, w_query, preferred_element_type=f32).astype(bf16)]
    all_to_all x2 -> x0, starting transfers between devices: 26.2 us -> none  [the longest x1 14.6 us: sent_to_all(): return lax.all_to_all(copies, axis, split_axis=0, concat_axis=0, tiled=True)]
    all_to_all x2 -> x0, waiting for transfers between devices: 12.6 us -> none  [the longest x1 8.78 us: summed_on_arrival(): parts = lax.all_to_all(split_up(shard, dim, count), axis, 0, 0, tiled=True)]
    convert_element_type x5 -> x8, other arithmetic: 2.66 us -> 7.48 us  [the longest x1 2.63 us: local(): latent = (raw * lax.rsqrt(jnp.mean(raw * raw, axis=0, keepdims=True) + ep...]
  transfers between devices with their start and end apart: 5 -> 1, of which waited for: 4 -> 0; matrix products, arithmetic and copies ran while one was open for 5% -> 14% of each run, Pallas kernels for 0% -> 6%
where the time goes in v1:
time: 142 us
  Pallas kernels  96.9 us (68%)
  other arithmetic  20.9 us (15%)
  local copies, waits for them, and re-layouts  12 us (8%)
  matrix products  6.67 us (5%)
  starting transfers between devices  3.75 us (3%)
  between operations  1.46 us (1%)
    pallas_call x4, Pallas kernels, kernel_call(): pl.pallas_call(functools.partial(body, sizes), out_shape=outs, in_specs=[...  87.9 us
    pallas_call x1, Pallas kernels, attention_call(): pl.pallas_call(functools.partial(attend, blocks, scale), grid=(total // r...  8.99 us
    unnamed x71, local copies, waits for them, and re-layouts  5.7 us
    ppermute x1, starting transfers between devices, local(): lax.ppermute(gated[plane - reach:], 'z', [(i, i + 1) for i in range(nz -...  3.75 us
  transfers between devices with their start and end apart: 1, of which 0 were waited for; matrix products, arithmetic and copies ran while one was open for 14% of the time, Pallas kernels for 6%

profile of v1, /device:TPU:1, one launch (start us, length us, event | category | flops | bytes accessed | tf_op | source)
XLA Modules:
  0.0 141.6 jit_solution(15006128204518145814)
XLA Ops:
  0.7 0.9 copy.34
  1.7 0.8 reshape.190
  2.5 0.8 reshape.191
  3.4 0.8 constant_dynamic-slice_fusion.1
  4.4 0.8 copy-done.4
  5.2 32.6 %gather_inputs.1 = (bf16[4,128,2048]{2,1,0:T(8,128)(2,1)S(1)}, bf16[72,2048]{1,0:T(8,128)(2,1)S(1)}, bf16[128,128]{1,0:T(8,128)(2,1)S(1)}) custom-call(bf16[128,256]{1,0:T(8,128)(2,1)S(1)} %copy-done.4, bf16[32,128]{1,0:T(8,128)(2,1)S(1)} %maximum_maximum_fusion.lw, bf16[4,32,128]{2,1,0:T(8,128)(2,1)S(1)} %maximum_bitcast_fusion.vg), custom_call_target="tpu_custom_call" | custom-call | tf_op jit(solution)/shard_map/gather_inputs/pallas_call | solution.py:361
  37.9 1.3 copy-done.3
  39.2 0.5 multiply_reduce_fusion.1
  39.7 2.1 %fusion.3 = bf16[512,2048]{1,0:T(8,128)(2,1)S(1)} fusion(f32[2048]{0:T(1024)S(1)} %copy-done.11, f32[512]{0:T(512)S(1)} %rsqrt_bitcast_fusion, bf16[4,128,2048]{2,1,0:T(8,128)(2,1)} %copy-done.3), kind=kLoop, calls=%fused_computation.5 | loop fusion | flops 4194304 | bytes 4204544 | tf_op jit(solution)/shard_map/convert_element_type | solution.py:502
  41.8 0.3 fusion.5
  42.2 0.1 fusion.55
  42.3 34.9 %gather_latent.1 = (bf16[8,72,2048]{2,1,0:T(8,128)(2,1)S(1)}, bf16[2048,128]{1,0:T(8,128)(2,1)S(1)}) custom-call(bf16[72,128]{1,0:T(8,128)(2,1)S(1)} %pad_maximum_fusion.2.own, bf16[128,128]{1,0:T(8,128)(2,1)S(1)} %get-tuple-element.15.vg), custom_call_target="tpu_custom_call" | custom-call | tf_op jit(solution)/shard_map/gather_latent/pallas_call | solution.py:361
  77.2 1.4 copy-done.1
  78.6 0.8 fusion.67
  79.5 0.6 copy-done.9
  80.1 0.7 slice.343
  80.8 3.7 %collective-permute-start = (bf16[30,64]{0,1:T(8,128)(2,1)}, bf16[30,64]{0,1:T(8,128)(2,1)}, u32[]{:S(2)}, u32[]{:S(2)}) collective-permute-start(bf16[30,64]{0,1:T(8,128)(2,1)} %slice.343), channel_id=1, source_target_pairs={{0,32},{32,64},{64,96},{96,128},{128,160},{160,192},{192,224},{224... | collective-permute-start | bytes 11528 | tf_op jit(solution)/shard_map/ppermute | solution.py:561
  84.6 0.5 multiply_power_fusion.1
  85.1 2.8 %multiply_reduce_fusion = f32[2048]{0:T(1024)} fusion(bf16[8,72,2048]{2,1,0:T(8,128)(2,1)} %copy-done.1), kind=kLoop, calls=%fused_computation.6 | loop fusion | flops 3143680 | bytes 2105344 | tf_op jit(solution)/shard_map/reduce_sum | solution.py:530
  87.9 1.0 slice.258
  88.9 2.5 %slice_convert_fusion = f32[8,64,2048]{2,1,0:T(8,128)} fusion(bf16[8,72,2048]{2,1,0:T(8,128)(2,1)S(1)} %copy-done.2), kind=kLoop, calls=%fused_computation.10 | loop fusion | flops 1048576 | bytes 6291456 | tf_op jit(solution)/shard_map/convert_element_type | solution.py:527
  91.4 0.6 add_convert_fusion.1
  92.1 0.7 slice_bitcast_fusion.30
  92.7 2.6 %convolution_convert_fusion.1 = bf16[512,384]{0,1:T(8,128)(2,1)S(1)} fusion(bf16[512,2048]{1,0:T(8,128)(2,1)} %copy-done.6, bf16[2048,384]{1,0:T(8,128)(2,1)S(1)} %copy-done), kind=kOutput, calls=%fused_computation.12 | convolution fusion | flops 805502976 | bytes 4063232 | tf_op jit(solution)/shard_map/dot_general | solution.py:539
  95.4 0.2 copy.49
  95.5 0.8 convert_element_type.96
  96.4 1.4 %convolution_convert_fusion = bf16[2,512,512]{2,1,0:T(8,128)(2,1)S(1)} fusion(bf16[512,2,192]{0,2,1:T(8,128)(2,1)S(1)} %bitcast.146, bf16[512,256]{1,0:T(8,128)(2,1)} %param.24), kind=kOutput, calls=%fused_computation.11 | convolution fusion | flops 134742016 | bytes 1572864 | tf_op jit(solution)/shard_map/thd,lhd->htl/dot_general | solution.py:551
  97.8 0.7 add_rsqrt_fusion
  98.8 1.7 %multiply_cosine_fusion = (f32[512,32]{1,0:T(8,128)S(1)}, f32[512,32]{1,0:T(8,128)S(1)}) fusion(f32[32]{0:T(128)} %multiply_power_fusion.1, f32[512]{0:T(512)} %add_convert_fusion.1), kind=kLoop, calls=%fused_computation.19 | loop fusion | flops 16384 | bytes 133248 | tf_op jit(solution)/shard_map/cos | solution.py:547
  100.5 1.4 %subtract_convert_fusion = (bf16[512,2,32]{2,0,1:T(8,128)(2,1)S(1)}, bf16[512,2,32]{2,0,1:T(8,128)(2,1)S(1)}) fusion(f32[512,2,64]{2,0,1:T(8,128)} %convert_element_type.96, f32[512,32]{1,0:T(8,128)S(1)} %get-tuple-element.69, f32[512,32]{1,0:T(8,128)S(1)} %get-tuple-element.68), kind=kLoop, calls=%fused_computation.17 | loop fusion | flops 262144 | bytes 524288 | tf_op jit(solution)/shard_map/convert.7
  101.9 0.1 pad_maximum_fusion
  102.1 2.6 %fusion.1.lat = bf16[512,2048]{1,0:T(8,128)(2,1)S(1)} fusion(f32[8,64,2048]{2,1,0:T(8,128)} %slice_convert_fusion, f32[512]{0:T(512)S(1)} %copy-done.13, f32[2048]{0:T(1024)S(1)} %add_rsqrt_fusion), kind=kLoop, calls=%fused_computation.2 | loop fusion | flops 3145728 | bytes 6301696 | tf_op jit(solution)/shard_map/convert_element_type | solution.py:532
  105.0 9.0 %attend.1 = (bf16[1024,128]{1,0:T(8,128)(2,1)S(1)}, f32[8,1024]{1,0:T(8,128)S(1)}) custom-call(bf16[1024,512]{1,0:T(8,128)(2,1)S(1)} %bitcast.138, bf16[1024,64]{1,0:T(8,128)(2,1)S(1)} %bitcast.139, bf16[512,2048]{1,0:T(8,128)(2,1)S(1)} %fusion.1.lat, bf16[64,2048]{1,0:T(8,128)(2,1)S(1)} %reshape.197.rope, bf16[512,256]{1,0:T(8,128)(2,1)S(1)} %copy-done.5), custom_call_target="tpu_custom_call" | custom-call | flops 4697620480 | bytes 6291456 | tf_op jit(solution)/shard_map/attend/pallas_call | solution.py:412
  114.0 0.8 maximum_convert_fusion
  115.0 1.5 %fusion.62 = (f32[512]{0:T(512)S(1)}, f32[512]{0:T(512)S(1)}, f32[512,64]{0,1:T(8,128)S(1)}) fusion(f32[542,64]{0,1:T(8,128)S(1)} %maximum_convert_fusion, f32[64]{0:T(128)S(1)} %copy-done.15, f32[64]{0:T(128)S(1)} %copy-done.16, f32[64]{0:T(128)S(1)} %copy-done.17, f32[64]{0:T(128)S(1)} %copy-done.18, f32[64]{0:T(128)S(1)} %copy-done.19, ...), kind=kLoop, calls=%fused_computation.169 | loop fusion | flops 2096128 | bytes 4206336 | tf_op jit(solution)/shard_map/reduce_sum | solution.py:585
  116.5 0.2 reshape.199
  116.7 0.2 fusion.65
  117.3 9.1 %exchange.1 = (bf16[4,2,128,128]{3,2,1,0:T(8,128)(2,1)S(1)}, f32[4,64,128]{2,1,0:T(8,128)S(1)}, f32[4,8,128]{2,1,0:T(8,128)S(1)}, f32[8,8,128]{2,1,0:T(8,128)S(1)}) custom-call(bf16[2,512,128]{2,1,0:T(8,128)(2,1)S(1)} %bitcast.140, f32[4,64,128]{2,1,0:T(8,128)S(1)} %pad_maximum_fusion.1.mixed, f32[4,8,128]{2,1,0:T(8,128)S(1)} %concatenate.35.st), custom_call_target="tpu_custom_call" | custom-call | tf_op jit(solution)/shard_map/exchange/pallas_call | solution.py:361
  126.5 0.6 add_bitcast_fusion
  127.0 0.2 multiply_reduce_fusion.2
  127.3 0.1 copy.47
  127.4 0.2 reshape.200
  127.6 0.2 copy.59
  127.8 0.2 reshape.201
  128.0 1.1 fusion.45
  129.2 0.3 fusion.4
  129.6 11.3 %scatter_rows.1 = bf16[8,16,2048]{2,1,0:T(8,128)(2,1)S(1)} custom-call(bf16[8,16,2048]{2,1,0:T(8,128)(2,1)S(1)} %bitcast.137), custom_call_target="tpu_custom_call" | custom-call | tf_op jit(solution)/shard_map/scatter_rows/pallas_call | solution.py:361
  140.9 0.7 reduce_sum.82
  (98 shorter events, 1.5 us)
Async XLA Ops:
  0.6 92.1 %copy-start = (bf16[2048,384]{1,0:T(8,128)(2,1)S(1)}, bf16[2048,384]{1,0:T(8,128)(2,1)}, u32[]{:S(2)}) copy-start(bf16[2048,384]{1,0:T(8,128)(2,1)} %param.20) | copy-start | bytes 4718596
  0.6 39.0 %copy-start.11 = (f32[2048]{0:T(1024)S(1)}, f32[2048]{0:T(1024)}, u32[]{:S(2)}) copy-start(f32[2048]{0:T(1024)} %param.15) | copy-start | bytes 24580
  4.4 0.8 copy-start.4
  37.9 1.3 copy-start.3
  41.8 37.6 %copy-start.6 = (bf16[512,2048]{1,0:T(8,128)(2,1)}, bf16[512,2048]{1,0:T(8,128)(2,1)S(1)}, u32[]{:S(2)}) copy-start(bf16[512,2048]{1,0:T(8,128)(2,1)S(1)} %fusion.3) | copy-start | bytes 6291460
  77.2 1.4 %copy-start.1 = (bf16[8,72,2048]{2,1,0:T(8,128)(2,1)}, bf16[8,72,2048]{2,1,0:T(8,128)(2,1)S(1)}, u32[]{:S(2)}) copy-start(bf16[8,72,2048]{2,1,0:T(8,128)(2,1)S(1)} %get-tuple-element.16) | copy-start | bytes 7077892
  79.5 0.6 copy-start.9
  80.8 33.2 %collective-permute-start = (bf16[30,64]{0,1:T(8,128)(2,1)}, bf16[30,64]{0,1:T(8,128)(2,1)}, u32[]{:S(2)}, u32[]{:S(2)}) collective-permute-start(bf16[30,64]{0,1:T(8,128)(2,1)} %slice.343), channel_id=1, source_target_pairs={{0,32},{32,64},{64,96},{96,128},{128,160},{160,192},{192,224},{224... | collective-permute-start | bytes 11528 | tf_op jit(solution)/shard_map/ppermute | solution.py:561
  84.6 4.3 %copy-start.2 = (bf16[8,72,2048]{2,1,0:T(8,128)(2,1)S(1)}, bf16[8,72,2048]{2,1,0:T(8,128)(2,1)}, u32[]{:S(2)}) copy-start(bf16[8,72,2048]{2,1,0:T(8,128)(2,1)} %copy-done.1) | copy-start | bytes 7077892
  88.9 3.1 %copy-start.12 = (bf16[31,256]{1,0:T(8,128)(2,1)S(1)}, bf16[31,256]{1,0:T(8,128)(2,1)}, u32[]{:S(2)}) copy-start(bf16[31,256]{1,0:T(8,128)(2,1)} %param.18) | copy-start | bytes 47620
  98.7 3.4 %copy-start.13 = (f32[512]{0:T(512)S(1)}, f32[512]{0:T(512)}, u32[]{:S(2)}) copy-start(f32[512]{0:T(512)} %param.22) | copy-start | bytes 6148
  102.1 2.6 %copy-start.5 = (bf16[512,256]{1,0:T(8,128)(2,1)S(1)}, bf16[512,256]{1,0:T(8,128)(2,1)}, u32[]{:S(2)}) copy-start(bf16[512,256]{1,0:T(8,128)(2,1)} %up.1) | copy-start | bytes 786436
  104.8 9.3 %copy-start.10 = (bf16[512,64]{0,1:T(8,128)(2,1)S(1)}, bf16[512,64]{0,1:T(8,128)(2,1)}, u32[]{:S(2)}) copy-start(bf16[512,64]{0,1:T(8,128)(2,1)} %copy-done.9) | copy-start | bytes 196612
  104.8 10.1 %copy-start.14 = (f32[64]{0:T(128)S(1)}, f32[64]{0:T(128)}, u32[]{:S(2)}) copy-start(f32[64]{0:T(128)} %get-tuple-element.37) | copy-start | bytes 772
  104.8 10.1 %copy-start.15 = (f32[64]{0:T(128)S(1)}, f32[64]{0:T(128)}, u32[]{:S(2)}) copy-start(f32[64]{0:T(128)} %get-tuple-element.38) | copy-start | bytes 772
  104.8 10.1 %copy-start.16 = (f32[64]{0:T(128)S(1)}, f32[64]{0:T(128)}, u32[]{:S(2)}) copy-start(f32[64]{0:T(128)} %get-tuple-element.39) | copy-start | bytes 772
  104.8 10.1 %copy-start.17 = (f32[64]{0:T(128)S(1)}, f32[64]{0:T(128)}, u32[]{:S(2)}) copy-start(f32[64]{0:T(128)} %get-tuple-element.40) | copy-start | bytes 772
  104.8 10.1 %copy-start.18 = (f32[64]{0:T(128)S(1)}, f32[64]{0:T(128)}, u32[]{:S(2)}) copy-start(f32[64]{0:T(128)} %get-tuple-element.41) | copy-start | bytes 772
  104.8 10.1 %copy-start.19 = (f32[64]{0:T(128)S(1)}, f32[64]{0:T(128)}, u32[]{:S(2)}) copy-start(f32[64]{0:T(128)} %get-tuple-element.42) | copy-start | bytes 772
  104.8 10.1 %copy-start.20 = (f32[64]{0:T(128)S(1)}, f32[64]{0:T(128)}, u32[]{:S(2)}) copy-start(f32[64]{0:T(128)} %get-tuple-element.43) | copy-start | bytes 772
  104.8 10.1 %copy-start.21 = (f32[64]{0:T(128)S(1)}, f32[64]{0:T(128)}, u32[]{:S(2)}) copy-start(f32[64]{0:T(128)} %get-tuple-element.44) | copy-start | bytes 772
  104.8 10.1 %copy-start.22 = (f32[64]{0:T(128)S(1)}, f32[64]{0:T(128)}, u32[]{:S(2)}) copy-start(f32[64]{0:T(128)} %get-tuple-element.45) | copy-start | bytes 772
  104.9 10.1 %copy-start.23 = (f32[64]{0:T(128)S(1)}, f32[64]{0:T(128)}, u32[]{:S(2)}) copy-start(f32[64]{0:T(128)} %get-tuple-element.46) | copy-start | bytes 772
  104.9 10.1 %copy-start.24 = (f32[64]{0:T(128)S(1)}, f32[64]{0:T(128)}, u32[]{:S(2)}) copy-start(f32[64]{0:T(128)} %get-tuple-element.47) | copy-start | bytes 772
  104.9 10.1 %copy-start.25 = (f32[64]{0:T(128)S(1)}, f32[64]{0:T(128)}, u32[]{:S(2)}) copy-start(f32[64]{0:T(128)} %get-tuple-element.48) | copy-start | bytes 772
  104.9 10.1 %copy-start.26 = (f32[64]{0:T(128)S(1)}, f32[64]{0:T(128)}, u32[]{:S(2)}) copy-start(f32[64]{0:T(128)} %get-tuple-element.49) | copy-start | bytes 772
  104.9 10.1 %copy-start.27 = (f32[64]{0:T(128)S(1)}, f32[64]{0:T(128)}, u32[]{:S(2)}) copy-start(f32[64]{0:T(128)} %get-tuple-element.50) | copy-start | bytes 772
  104.9 10.1 %copy-start.28 = (f32[64]{0:T(128)S(1)}, f32[64]{0:T(128)}, u32[]{:S(2)}) copy-start(f32[64]{0:T(128)} %get-tuple-element.51) | copy-start | bytes 772
  104.9 10.1 %copy-start.29 = (f32[64]{0:T(128)S(1)}, f32[64]{0:T(128)}, u32[]{:S(2)}) copy-start(f32[64]{0:T(128)} %get-tuple-element.52) | copy-start | bytes 772
  104.9 10.1 %copy-start.30 = (f32[64]{0:T(128)S(1)}, f32[64]{0:T(128)}, u32[]{:S(2)}) copy-start(f32[64]{0:T(128)} %get-tuple-element.53) | copy-start | bytes 772
  104.9 10.1 %copy-start.31 = (f32[64]{0:T(128)S(1)}, f32[64]{0:T(128)}, u32[]{:S(2)}) copy-start(f32[64]{0:T(128)} %get-tuple-element.54) | copy-start | bytes 772
  104.9 10.1 %copy-start.32 = (f32[64]{0:T(128)S(1)}, f32[64]{0:T(128)}, u32[]{:S(2)}) copy-start(f32[64]{0:T(128)} %get-tuple-element.55) | copy-start | bytes 772
  116.5 11.5 %copy-start.7 = (bf16[256,2048]{1,0:T(8,128)(2,1)S(1)}, bf16[256,2048]{1,0:T(8,128)(2,1)}, u32[]{:S(2)}) copy-start(bf16[256,2048]{1,0:T(8,128)(2,1)} %param.26) | copy-start | bytes 3145732
  128.0 1.2 copy-start.8

commit v2 on v0

v2 whole, which is shorter than its diff:
```python
import functools

import jax
import jax.numpy as jnp
import numpy as np
import numpy as np
import numpy as np
from jax import lax
from jax.experimental import pallas as pl
from jax.experimental.pallas import tpu as pltpu
from jax.sharding import Mesh
from jax.sharding import PartitionSpec as P

PLAIN_QK_WIDTH = 128
QK_ROPE = 64
VALUE_HEAD_WIDTH = 128
epsilon = 1e-06
rope_base = 10000.0
masked_score = -1e30
SP = ("z", "y")
TP = ("x", "c")
LANES = 128
VMEM = pl.BlockSpec(memory_space=pltpu.VMEM)
MIB = 1 << 20


class Net:
    def __init__(self, sizes, send, recv):
        self.nz, self.ny, self.nx, self.nc = sizes
        self.z, self.y, self.x, self.c = (lax.axis_index(a) for a in ("z", "y", "x", "c"))
        self.send, self.recv = send, recv
        self.ids, self.open = {}, []

    def number(self, name):
        return self.ids.setdefault(name, len(self.ids))

    def put(self, name, src, dst, **to):
        k = self.number(name)
        copy = pltpu.make_async_remote_copy(
            src_ref=src,
            dst_ref=dst,
            send_sem=self.send.at[k],
            recv_sem=self.recv.at[k],
            device_id=to,
            device_id_type=pl.DeviceIdType.MESH,
        )
        copy.start()
        self.open.append(copy)

    def got(self, name, dst, **to):
        k = self.number(name)
        pltpu.make_async_remote_copy(
            src_ref=dst,
            dst_ref=dst,
            send_sem=self.send.at[k],
            recv_sem=self.recv.at[k],
            device_id=to,
            device_id_type=pl.DeviceIdType.MESH,
        ).wait_recv()

    def finish(self):
        for copy in self.open:
            copy.wait_send()

    def zp(self, d):
        return lax.rem(self.z + d + self.nz, self.nz)

    def yp(self, d):
        return lax.rem(self.y + d + self.ny, self.ny)

    def xp(self, d):
        return lax.rem(self.x + d + self.nx, self.nx)

    def cp(self):
        return 1 - self.c

    def greet(self, peers):
        barrier = pltpu.get_barrier_semaphore()
        for to in peers:
            pl.semaphore_signal(barrier, inc=1, device_id=to, device_id_type=pl.DeviceIdType.MESH)
        pl.semaphore_wait(barrier, len(peers))


def z_plan(nz):
    group = 4 if nz >= 16 else 2
    count = nz // group
    if group == 4:
        near = {1: range(count), -1: range(count), 2: (0, 1), -2: (1, 2)}
    else:
        near = {1: range(count)}
    return group, count, near


def z_order(nz):
    group, count, near = z_plan(nz)
    order = [0] + [group * b for b in ((1, 3, 2) if count == 4 else range(1, count))]
    for b in (0, 1, 3, 2) if count == 4 else range(count):
        for d, blocks in near.items():
            if b in blocks:
                order.append((b * group - d) % nz)
    return order


def z_peers(net):
    group, count, near = z_plan(net.nz)
    far = (1, -1) if count > 2 else (1,) if count == 2 else ()
    peers = [{"z": net.zp(d)} for d in [group * f for f in far] + list(near)]
    if group == 2:
        peers.append({"z": net.zp(-1)})
    return peers


class ZGather:
    def __init__(self, net, tag, here, there):
        self.net, self.tag, self.here, self.there = net, tag, here, there
        self.group, self.count, self.near = z_plan(net.nz)
        z_class = net.z // self.group
        self.turn = jnp.where(lax.rem(z_class, 2) == 1, 1, -1)

    def start(self):
        n, g = self.net, self.group
        if self.count >= 2:
            n.put((self.tag, "f", 1), self.here(0), self.there(0, g), z=n.zp(g))
        if self.count > 2:
            n.put((self.tag, "f", -1), self.here(0), self.there(0, -g), z=n.zp(-g))
        self.spread(0)

    def spread(self, b):
        n = self.net
        k = b * self.group
        for d, blocks in self.near.items():
            if b in blocks:
                n.put((self.tag, "n", d, b), self.here(k), self.there(k, d), z=n.zp(d))

    def far_first(self):
        n, g = self.net, self.group
        if self.count == 2:
            n.got((self.tag, "f", 1), self.here(g), z=n.zp(g))
            self.spread(1)
            return [g]
        n.got((self.tag, "f", 1), self.here(3 * g), z=n.zp(g))
        n.got((self.tag, "f", -1), self.here(g), z=n.zp(g))
        n.put(
            (self.tag, "r"), self.here(-g * self.turn), self.there(-g * self.turn, g * self.turn),
            z=n.zp(g * self.turn),
        )
        self.spread(1)
        self.spread(3)
        return [g, 3 * g]

    def far_last(self):
        n, g = self.net, self.group
        if self.count == 2:
            return []
        n.got((self.tag, "r"), self.here(2 * g), z=n.zp(g))
        self.spread(2)
        return [2 * g]

    def close(self, picked=None):
        n, g = self.net, self.group
        for b in (0, 1, 3, 2) if self.count == 4 else range(self.count):
            for d, blocks in self.near.items():
                if b in blocks and (picked is None or b in picked):
                    at = (b * g - d) % n.nz
                    n.got((self.tag, "n", d, b), self.here(at), z=n.zp(d))
                    yield at


def tile(i, size):
    return pl.ds(pl.multiple_of(i * size, size), size)


def turned(v, shift):
    return pltpu.roll(v, shift, 1)


def layer(
    sizes, tok, wv, wg, wl, wr, gain, lgain, taps, cgain, invq, invk, wq_h, ku_h, vu_h, wc_h, wa_h,
    merged, logs,
    X, N, WL, VG, W, yb, lw, vg, wide, K, LA, QA, M, L, ACC, G, MX, ATT, CS, ML, LG,
    att_r, mix_r, cs_r, ml_r, stat_r, CP, PART, parts_r,
    wq, ku, vu, wc, wa, load, send, recv,
):
    f32, bf16 = jnp.float32, jnp.bfloat16
    net = Net(sizes, send, recv)
    nz, ny, nx, nc = sizes
    ntp = nx * nc
    z, y, x, c = net.z, net.y, net.x, net.c
    o = net.cp()
    j = x * nc + c
    rows, feats = tok.shape
    half = feats // 2
    width = X.shape[1]
    plane = rows * ny
    wrows = wv.shape[0]
    rank = lgain.shape[1]
    lat_share = rank // ntp
    rope_share = QK_ROPE // ntp
    pairs = rope_share // 2
    kept = lat_share + rope_share
    share = wv.shape[1] // ny
    heads = vu.shape[1] // VALUE_HEAD_WIDTH
    keys = nz * rows
    mid = rows // 2

    loads = []
    for k, (src, dst) in enumerate(((wq_h, wq), (ku_h, ku), (vu_h, vu), (wc_h, wc), (wa_h, wa))):
        loads.append(pltpu.make_async_copy(src, dst, load.at[k]))
        loads[-1].start()

    offsets = [(a, b) for a in range(nx) for b in range(nc) if a or b]

    def there(a, b):
        return {"x": net.xp(a), "c": c if b == 0 else o}

    peers = [{"y": net.yp(k)} for k in range(1, ny)] + [there(a, b) for a, b in offsets]
    peers += z_peers(net)
    barrier = pltpu.get_barrier_semaphore()
    for to in peers:
        pl.semaphore_signal(barrier, inc=1, device_id=to, device_id_type=pl.DeviceIdType.MESH)

    lane = lax.broadcasted_iota(jnp.int32, (wrows, LANES), 1)
    low = lane < share
    for t in range(ny):
        v = wv[:, t // 2 * LANES : (t // 2 + 1) * LANES].astype(f32)
        g = wg[:, t // 2 * LANES : (t // 2 + 1) * LANES].astype(f32)
        v, g = (v, turned(g, share)) if t % 2 == 0 else (turned(v, share), g)
        vg[t] = jnp.where(low, v, g).astype(bf16)
    lat = wl[:, tile(j // 2, LANES)].astype(f32)
    lat = jnp.where(lax.rem(j, 2) == 0, lat, turned(lat, lat_share))
    wide[...] = jnp.zeros(wide.shape, f32)
    wide[:, :QK_ROPE] = wr[...].astype(f32)
    rope = wide[...]
    rope_a = turned(rope, lat_share - pairs * j)
    rope_b = turned(rope, LANES + lat_share + pairs - QK_ROPE // 2 - pairs * j)
    lw[...] = jnp.where(
        lane < lat_share, lat, jnp.where(lane < lat_share + pairs, rope_a, rope_b)
    ).astype(bf16)
    yb[pl.ds(y, 1)] = lw[...][None]
    VG[tile(y, wrows)] = vg[pl.ds(y, 1)].reshape(vg.shape[1:])

    pl.semaphore_wait(barrier, len(peers))

    def cols(side, xx, cc):
        return tile((xx * nc + cc) * 2 + side, half)

    def place(side, yy, xx, cc):
        return X.at[tile(yy, rows), cols(side, xx, cc)]

    mine = [tok.at[:, pl.ds(0, half)], tok.at[:, pl.ds(half, half)]]
    for k in range(1, ny):
        net.put(("lw", k), lw, yb.at[y], y=net.yp(k))
    for k in range(1, ny):
        net.put(("ya", k), mine[0], place(0, y, x, c), y=net.yp(k))
    for k in range(1, nx):
        net.put(("xb", k), mine[1], place(1, y, x, c), x=net.xp(k))
    for k in range(1, nx):
        net.put(("xa", 0, k), mine[0], place(0, y, x, c), x=net.xp(k))
    for k in range(1, ny):
        net.put(("vg", k), vg.at[net.yp(k)], VG.at[tile(y, wrows)], y=net.yp(k))
    for k in range(1, ny):
        net.put(("yb", 0, k), mine[1], place(1, y, x, c), y=net.yp(k))
    for side in (0, 1):
        net.put(("s", side), mine[side], place(side, y, x, c), c=o)
        X[tile(y, rows), cols(side, x, c)] = tok[:, side * half : (side + 1) * half]

    for k in range(1, ny):
        net.got(("lw", k), yb.at[net.yp(-k)], y=net.yp(k))
    WL[:, tile(z, LANES)] = yb[...].reshape(ny * wrows, LANES).astype(f32).T[:kept].astype(bf16)
    zg = ZGather(
        net, "wl", lambda n: WL.at[:, tile(net.zp(n), LANES)],
        lambda n, d: WL.at[:, tile(net.zp(n), LANES)],
    )
    zg.start()

    for k in range(1, ny):
        at = place(0, net.yp(-k), x, c)
        net.got(("ya", k), at, y=net.yp(k))
        for i in range(1, nx):
            net.put(("xa", k, i), at, at, x=net.xp(i))
        net.put(("sa", k), at, at, c=o)
    for k in range(1, nx):
        at = place(1, y, net.xp(-k), c)
        net.got(("xb", k), at, x=net.xp(k))
        for i in range(1, ny):
            net.put(("yb", k, i), at, at, y=net.yp(i))
        net.put(("sb", k), at, at, c=o)
    for k in range(1, ny):
        net.got(("vg", k), VG.at[tile(net.yp(-k), wrows)], y=net.yp(k))
    depth = ny * wrows
    W[tile(z, depth)] = VG[...]
    zw = ZGather(
        net, "w", lambda n: W.at[tile(net.zp(n), depth)], lambda n, d: W.at[tile(net.zp(n), depth)]
    )
    zw.start()
    zg.far_first()
    for k in range(ny):
        for i in range(1, nx):
            at = place(0, net.yp(-k), net.xp(-i), c)
            net.got(("xa", k, i), at, x=net.xp(i))
            net.put(("sxa", k, i), at, at, c=o)
    for k in range(nx):
        for i in range(1, ny):
            at = place(1, net.yp(-i), net.xp(-k), c)
            net.got(("yb", k, i), at, y=net.yp(i))
            net.put(("syb", k, i), at, at, c=o)
    zw.far_first()
    zg.far_last()
    for side in (0, 1):
        net.got(("s", side), place(side, y, x, o), c=o)
    for k in range(1, ny):
        net.got(("sa", k), place(0, net.yp(-k), x, o), c=o)
    for k in range(1, nx):
        net.got(("sb", k), place(1, y, net.xp(-k), o), c=o)
    for k in range(ny):
        for i in range(1, nx):
            net.got(("sxa", k, i), place(0, net.yp(-k), net.xp(-i), o), c=o)
    for k in range(nx):
        for i in range(1, ny):
            net.got(("syb", k, i), place(1, net.yp(-i), net.xp(-k), o), c=o)

    piece = min(64, rows)

    def norm_rows(i, _):
        at = tile(i, piece)
        v = X[at, :].astype(f32)
        v = v * lax.rsqrt(jnp.mean(v * v, axis=1, keepdims=True) + epsilon) * gain[...]
        N[at, :] = v.astype(bf16)
        return _

    lax.fori_loop(0, plane // piece, norm_rows, 0)
    zw.far_last()

    loads[0].wait()
    loads[1].wait()
    band = min(128, plane)

    def query_rows(i, _):
        at = tile(i, band)
        q = jnp.dot(N[at, :], wq[...], preferred_element_type=f32).astype(bf16).astype(f32)
        lanes = lax.broadcasted_iota(jnp.int32, (band, LANES), 1)
        first_head = lanes < QK_ROPE
        b, d = q[:, LANES : 2 * LANES], q[:, 2 * LANES :]
        plain = (
            q[:, :LANES],
            jnp.where(first_head, turned(b, QK_ROPE), turned(d, QK_ROPE)),
        )
        rot = jnp.where(first_head, b, d)
        pos = z * plane + i * band + lax.broadcasted_iota(jnp.int32, (band, LANES), 0)
        ang = pos.astype(f32) * invq[...]
        front = lax.rem(lanes, QK_ROPE) < QK_ROPE // 2
        swap = jnp.where(front, turned(rot, LANES - QK_ROPE // 2), turned(rot, QK_ROPE // 2))
        sine = jnp.sin(ang)
        rot = rot * jnp.cos(ang) + swap * jnp.where(front, -sine, sine)
        for h in range(heads):
            ql = lax.dot_general(
                plain[h].astype(bf16), ku[:, h * LANES : (h + 1) * LANES],
                (((1,), (1,)), ((), ())), preferred_element_type=f32,
            )
            to = tile(h * (plane // band) + i, band)
            QA[to, :rank] = ql.astype(bf16)
            QA[to, rank:] = jnp.where(first_head == (h == 0), rot, 0.0).astype(bf16)
        return _

    lax.fori_loop(0, plane // band, query_rows, 0)
    for _ in zg.close():
        pass

    pre = lax.dot_general(
        WL[...], N[tile(y, rows), :], (((1,), (1,)), ((), ())), preferred_element_type=f32
    )
    angle = (
        (z * plane + y * rows + lax.broadcasted_iota(jnp.int32, (rope_share, rows), 1)).astype(f32)
        * invk[tile(j, rope_share), :rows]
    )
    part = pre[lat_share:]
    second = lax.broadcasted_iota(jnp.int32, (rope_share, rows), 0) >= pairs
    other = pltpu.roll(part, pairs, 0)
    part = part * jnp.cos(angle) + other * jnp.where(second, jnp.sin(angle), -jnp.sin(angle))

    order = z_order(nz)
    spot = {n: k for k, n in enumerate(order)}

    def slot(n, jj=None):
        if isinstance(n, int):
            at = pl.ds(spot[n % nz] * rows, rows)
        else:
            g = z_plan(nz)[0]
            at = tile(jnp.where(n > 0, spot[g], spot[nz - g]), rows)
        return K.at[j if jj is None else jj, :, at]

    def slot_there(n, d):
        if isinstance(n, int):
            return slot(n - d)
        return slot(2 * z_plan(nz)[0])

    K[pl.ds(j, 1), :lat_share, :rows] = pre[:lat_share].astype(bf16)[None]
    K[pl.ds(j, 1), lat_share:, :rows] = part.astype(bf16)[None]
    zl = ZGather(net, "l", slot, slot_there)

    def onward(n):
        for k in range(1, nx):
            net.put(("x", n, k), slot(n), slot(n), x=net.xp(k))
        net.put(("ls", n), slot(n), slot(n), c=o)

    zl.start()
    onward(0)
    LG[...] = jnp.broadcast_to(lgain[...], (rows, rank)).T
    for _ in zw.close():
        pass
    @pl.when(z == 0)
    def _():
        G[:32] = jnp.zeros((32, LANES), f32)

    def gated_rows(i, _):
        both = jnp.dot(N[tile(i, band), :], W[...], preferred_element_type=f32)
        gate = turned(both, share)
        g = both * jax.nn.sigmoid(gate)
        G[pl.ds(pl.multiple_of(32 + i * band, 8), band), :] = g.astype(bf16).astype(f32)
        return _

    lax.fori_loop(0, plane // band, gated_rows, 0)
    @pl.when(z < nz - 1)
    def _():
        k = net.number(("halo",))
        pltpu.make_async_remote_copy(
            src_ref=G.at[pl.ds(plane, 32)], dst_ref=G.at[pl.ds(0, 32)],
            send_sem=send.at[k], recv_sem=recv.at[k],
            device_id={"z": net.zp(1)}, device_id_type=pl.DeviceIdType.MESH,
        ).start()

    def arrive(ns):
        for n in ns:
            for k in range(1, nx):
                at = slot(n, net.xp(-k) * nc + c)
                net.got(("x", n, k), at, x=net.xp(k))
                net.put(("sx", n, k), at, at, c=o)

    def sibling(ns):
        for n in ns:
            net.got(("ls", n), slot(n, x * nc + o), c=o)
            for k in range(1, nx):
                net.got(("sx", n, k), slot(n, net.xp(-k) * nc + o), c=o)

    def keys_of(first, count):
        for s in range(first, first + count):
            at = pl.ds(s * rows, rows)
            raw = [K[t, :lat_share, at].astype(f32) for t in range(ntp)]
            total = sum(jnp.sum(r * r, axis=0, keepdims=True) for r in raw)
            scale = lax.rsqrt(total / rank + epsilon)
            for t in range(ntp):
                span = slice(t * lat_share, (t + 1) * lat_share)
                LA[span, at] = (raw[t] * scale * LG[span]).astype(bf16)
            r = [K[t, lat_share:, at].astype(f32) for t in range(ntp)]
            if pairs == 4:
                upper = lax.broadcasted_iota(jnp.int32, (8, rows), 0) < 4
                lo = [
                    jnp.where(upper, r[t], pltpu.roll(r[t + 1], 4, 0)) for t in range(0, ntp, 2)
                ]
                hi = [
                    jnp.where(upper, pltpu.roll(r[t], 4, 0), r[t + 1]) for t in range(0, ntp, 2)
                ]
            else:
                lo, hi = [v[:pairs] for v in r], [v[pairs:] for v in r]
            rot = jnp.concatenate(lo + hi, axis=0).astype(bf16)
            LA[rank : rank + QK_ROPE, at] = rot
            LA[rank + QK_ROPE :, at] = rot

    score_scale = (PLAIN_QK_WIDTH + QK_ROPE) ** (-0.5)

    def attend(first, count, h, fresh):
        at = pl.ds(first * rows, count * rows)
        to = pl.ds(h * plane, plane)
        lanes = lax.broadcasted_iota(jnp.int32, (1, count * rows), 1)
        key_at = jnp.zeros((1, count * rows), jnp.int32)
        for s in range(count):
            base = net.zp(order[first + s]) * plane + y * rows - s * rows
            key_at = jnp.where(lanes >= s * rows, base + lanes, key_at)
        query_at = z * plane + lax.broadcasted_iota(jnp.int32, (plane, 1), 0)
        s = jnp.dot(QA[to, :], LA[:, at], preferred_element_type=f32)
        s = jnp.where(key_at <= query_at, s * score_scale, masked_score)
        top = jnp.max(s, axis=1, keepdims=True)
        old = masked_score * 0.1 if fresh else M[to, :1]
        top = jnp.maximum(old, top)
        w = jnp.exp(s - top)
        total = jnp.sum(w, axis=1, keepdims=True)
        part = lax.dot_general(
            w.astype(bf16), LA[:rank, at], (((1,), (1,)), ((), ())), preferred_element_type=f32
        )
        if fresh:
            L[to, :] = jnp.broadcast_to(total, (plane, LANES))
            ACC[to, :] = part
        else:
            keep = jnp.exp(old - top)
            L[to, :] = L[to, :] * keep + total
            ACC[to, :] = ACC[to, :] * keep + part
        M[to, :] = jnp.broadcast_to(top, (plane, LANES))

    early, late = order[: max(1, nz // 4)], order[max(1, nz // 4) :]
    for n in zl.far_first():
        onward(n)

    @pl.when(z > 0)
    def _():
        k = net.number(("halo",))
        pltpu.make_async_remote_copy(
            src_ref=G.at[pl.ds(0, 32)], dst_ref=G.at[pl.ds(0, 32)],
            send_sem=send.at[k], recv_sem=recv.at[k],
            device_id={"z": net.zp(1)}, device_id_type=pl.DeviceIdType.MESH,
        ).wait_recv()

    reach = taps.shape[0] - 1
    t = taps[:, tile(y // 2, LANES)].astype(f32)
    low = lax.broadcasted_iota(jnp.int32, t.shape, 1) < share
    t = jnp.where(low == (lax.rem(y, 2) == 0), t, turned(t, share))
    low = lax.broadcasted_iota(jnp.int32, (mid, LANES), 1) < share
    for t_y in range(ny):
        lo = G[pl.ds(t_y * rows, mid + 32), :]
        hi = turned(G[pl.ds(t_y * rows + mid, mid + 32), :], share)
        wide = lax.broadcasted_iota(jnp.int32, (mid + 32, LANES), 1) < share
        both = jnp.where(wide, lo, hi)
        mixed = jnp.zeros((mid, LANES), f32)
        for k in range(reach + 1):
            off = 32 - reach + k
            mixed = mixed + t[k : k + 1] * both[off : off + mid]
        MX[t_y] = mixed
        spread = lax.broadcasted_iota(jnp.int32, (rows, LANES), 1)
        cs = jnp.zeros((rows, LANES), f32)
        for r, v in enumerate((mixed, mixed * mixed)):
            v = jnp.concatenate(
                [
                    jnp.sum(jnp.where(low, v, 0.0), axis=1, keepdims=True),
                    jnp.sum(jnp.where(low, 0.0, v), axis=1, keepdims=True),
                ],
                axis=0,
            )
            cs = jnp.where(spread == r, v, cs)
        CS[t_y] = cs.T[:8]
    for k in range(1, ny):
        to = net.yp(k)
        net.put(("cs", k), CS.at[to], cs_r.at[y], y=to)
    for k in range(1, ny):
        to = net.yp(k)
        net.put(("m", k), MX.at[to], mix_r.at[y], y=to)
    mix_r[pl.ds(y, 1)] = MX[pl.ds(y, 1)]
    cs_r[pl.ds(y, 1)] = CS[pl.ds(y, 1)]

    for n in zl.far_last():
        onward(n)
    for n in zl.close():
        onward(n)

    arrive(early)
    sibling(early)
    keys_of(0, len(early))
    for h in range(heads):
        attend(0, len(early), h, True)

    for k in range(1, ny):
        net.got(("cs", k), cs_r.at[net.yp(-k)], y=net.yp(k))
    stat_r[pl.ds(j, 1)] = sum(cs_r[k] for k in range(ny))[None]
    for a, b in offsets:
        net.put(("t", a, b), stat_r.at[j], stat_r.at[j], **there(a, b))
    for k in range(len(late)):
        arrive(late[k : k + 1])
        if k:
            sibling(late[k - 1 : k])
            keys_of(len(early) + k - 1, 1)

    def column(r):
        return jnp.broadcast_to(r, (LANES, rows)).T

    for k in range(1, ny):
        net.got(("m", k), mix_r.at[net.yp(-k)], y=net.yp(k))
    for a, b in offsets:
        jj = net.xp(-a) * nc + (c if b == 0 else o)
        net.got(("t", a, b), stat_r.at[jj], **there(a, b))
    stats = sum(stat_r[k] for k in range(ntp))
    channels = share * ny * ntp
    mean = stats[0:1] / channels
    var = stats[1:2] / channels - mean * mean
    mean, inv = column(mean), column(lax.rsqrt(var + epsilon))
    pieces = []
    for p in range(ny // 2):
        m0, m1 = mix_r[2 * p], mix_r[2 * p + 1]
        v = jnp.concatenate(
            [jnp.where(low, m0, turned(m1, share)), jnp.where(low, turned(m0, share), m1)], axis=0
        )
        v = (v - mean) * inv * cgain[:, p * LANES : (p + 1) * LANES]
        pieces.append((v * jax.nn.sigmoid(v)).astype(bf16))
    conv_out = jnp.concatenate(pieces, axis=1)
    for k in range(2, 5):
        loads[k].wait()
    cut = min(512, width)
    for k in range(width // cut):
        at = slice(k * cut, (k + 1) * cut)
        CP[:, at] = jnp.dot(conv_out, wc[:, at], preferred_element_type=f32)
    sibling(late[-1:])
    keys_of(nz - 1, 1)

    spread = lax.broadcasted_iota(jnp.int32, (rows, LANES), 1)
    for h in range(heads):
        attend(len(early), len(late), h, False)
        span = pl.ds(h * plane, plane)
        for t_y in range(ny):
            at = pl.ds(h * plane + t_y * rows, rows)
            ML[h, t_y] = jnp.where(spread == 0, M[at, :], L[at, :]).T[:8]
        for k in range(1, ny):
            to = net.yp(k)
            net.put(("ml", k, h), ML.at[h, to], ml_r.at[h, y], y=to)
        mean = (ACC[span, :] / jnp.maximum(L[span, :1], 1e-30)).astype(bf16)
        ATT[span, :] = jnp.dot(
            mean, vu[:, h * VALUE_HEAD_WIDTH : (h + 1) * VALUE_HEAD_WIDTH],
            preferred_element_type=f32,
        ).astype(bf16)
        for k in range(1, ny):
            to = net.yp(k)
            net.put(("a", k, h), ATT.at[tile(h * ny + to, rows), :], att_r.at[y, h], y=to)
        att_r[pl.ds(y, 1), h] = ATT[tile(h * ny + y, rows), :][None]
        ml_r[h, pl.ds(y, 1)] = ML[h, pl.ds(y, 1)]

    out, log_rows = [], []
    for h in range(heads):
        for k in range(1, ny):
            net.got(("ml", k, h), ml_r.at[h, net.yp(-k)], y=net.yp(k))
        tops = [ml_r[h, k, 0:1] for k in range(ny)]
        top = functools.reduce(jnp.maximum, tops)
        f = [jnp.exp(tops[k] - top) * ml_r[h, k, 1:2] for k in range(ny)]
        total = sum(f)
        log_rows.append(top + jnp.log(total))
        f = [column(v / total) for v in f]
        for k in range(1, ny):
            net.got(("a", k, h), att_r.at[net.yp(-k), h], y=net.yp(k))
        out.append(sum(f[k] * att_r[k, h].astype(f32) for k in range(ny)).astype(bf16))
    attention = jnp.concatenate(out, axis=1)
    logs[...] = jnp.concatenate(log_rows, axis=0)
    final = rows // ntp
    for k in range(width // cut):
        at = slice(k * cut, (k + 1) * cut)
        part = CP[:, at] + jnp.dot(attention, wa[:, at], preferred_element_type=f32)
        PART[:, at] = part.astype(bf16)
    for a, b in offsets:
        to = there(a, b)
        net.put(("p", a, b), PART.at[tile(to["x"] * nc + to["c"], final), :], parts_r.at[j], **to)
    total = PART[tile(j, final), :].astype(f32)
    for a, b in sorted(offsets, key=lambda v: min(v[0], nx - v[0])):
        source = there(-a, b)
        jj = source["x"] * nc + source["c"]
        net.got(("p", a, b), parts_r.at[jj], **there(a, b))
        total = total + parts_r[jj].astype(f32)
    merged[...] = total.astype(bf16)
    net.finish()

    @pl.when(z < nz - 1)
    def _():
        k = net.number(("halo",))
        pltpu.make_async_remote_copy(
            src_ref=G.at[pl.ds(plane, 32)], dst_ref=G.at[pl.ds(0, 32)],
            send_sem=send.at[k], recv_sem=recv.at[k],
            device_id={"z": net.zp(1)}, device_id_type=pl.DeviceIdType.MESH,
        ).wait_send()


def hand_on(a, b, a_out, b_out):
    a_out[...] = a[...]
    b_out[...] = b[...]


def local(
    tokens,
    norm_gain,
    w_value,
    w_gate,
    conv_taps,
    conv_gain,
    w_query,
    latent_down_weight,
    latent_norm_gain,
    w_rope_key,
    key_up_weight,
    value_up_weight,
    w_merge_conv,
    w_merge_attn,
):
    bf16, f32 = jnp.bfloat16, jnp.float32
    sizes = nz, ny, nx, nc = tuple(lax.axis_size(a) for a in ("z", "y", "x", "c"))
    ntp = nx * nc
    rows, feats = tokens.shape
    width = feats * ntp
    plane, keys = rows * ny, rows * nz
    wrows, chans = w_value.shape
    rank = latent_down_weight.shape[1]
    pairs = QK_ROPE // ntp // 2
    kept = rank // ntp + 2 * pairs
    heads = key_up_weight.shape[1] // PLAIN_QK_WIDTH
    mid = rows // 2
    middle = QK_ROPE // 2

    rates = np.float32(rope_base) ** (-2.0 * np.arange(middle, dtype=np.float32) / QK_ROPE)
    rates = rates.astype(np.float32)
    invq = jnp.asarray(np.tile(rates, LANES // middle)[None])
    by_row = [rates[t * pairs + i % pairs] for t in range(ntp) for i in range(2 * pairs)]
    invk = jnp.asarray(np.repeat(np.array(by_row, np.float32)[:, None], LANES, axis=1))

    args = (
        tokens, w_value, w_gate, latent_down_weight, w_rope_key, norm_gain[None], latent_norm_gain[None],
        conv_taps, conv_gain[None], invq, invk,
        w_query, key_up_weight, value_up_weight, w_merge_conv, w_merge_attn,
    )
    anywhere = pl.BlockSpec(memory_space=pl.ANY)
    messages = 400
    vm = pltpu.VMEM
    total = heads * plane
    scratch = [
        vm((plane, width), bf16),
        vm((plane, width), bf16),
        vm((kept, nz * LANES), bf16),
        vm((ny * wrows, LANES), bf16),
        vm((nz * ny * wrows, LANES), bf16),
        vm((ny, wrows, LANES), bf16),
        vm((wrows, LANES), bf16),
        vm((ny, wrows, LANES), bf16),
        vm((wrows, LANES), f32),
        vm((ntp, kept, keys), bf16),
        vm((rank + LANES, keys), bf16),
        vm((total, rank + LANES), bf16),
        vm((total, LANES), f32),
        vm((total, LANES), f32),
        vm((total, rank), f32),
        vm((plane + 32, LANES), f32),
        vm((ny, mid, LANES), f32),
        vm((total, VALUE_HEAD_WIDTH), bf16),
        vm((ny, 8, rows), f32),
        vm((heads, ny, 8, rows), f32),
        vm((rank, rows), f32),
        vm((ny, heads, rows, VALUE_HEAD_WIDTH), bf16),
        vm((ny, mid, LANES), f32),
        vm((ny, 8, rows), f32),
        vm((heads, ny, 8, rows), f32),
        vm((ntp, 8, rows), f32),
        vm((rows, width), f32),
        vm((rows, width), bf16),
        vm((ntp, rows // ntp, width), bf16),
        vm(w_query.shape, bf16),
        vm(key_up_weight.shape, bf16),
        vm(value_up_weight.shape, bf16),
        vm(w_merge_conv.shape, bf16),
        vm(w_merge_attn.shape, bf16),
        pltpu.SemaphoreType.DMA((5,)),
        pltpu.SemaphoreType.DMA((messages,)),
        pltpu.SemaphoreType.DMA((messages,)),
    ]
    result = pl.pallas_call(
        functools.partial(layer, sizes),
        out_shape=[
            jax.ShapeDtypeStruct((rows // ntp, width), bf16),
            jax.ShapeDtypeStruct((heads, rows), f32),
        ],
        in_specs=[VMEM] * 11 + [anywhere] * 5,
        out_specs=[VMEM, VMEM],
        scratch_shapes=scratch,
        compiler_params=pltpu.CompilerParams(
            collective_id=0, has_side_effects=True, vmem_limit_bytes=56 * MIB
        ),
        name="layer",
    )(*args)
    merged, logs = (
        pl.pallas_call(
            hand_on,
            out_shape=[jax.ShapeDtypeStruct(r.shape, r.dtype) for r in result],
            in_specs=[VMEM, VMEM],
            out_specs=[VMEM, VMEM],
            compiler_params=pltpu.CompilerParams(vmem_limit_bytes=MIB),
            name="hand_on",
        )(*result)
    )
    return merged, logs.T


def solution(mesh):
    devices = mesh.devices
    shape = (devices.shape[0] // 4, 4, 4, 2)
    finer = Mesh(devices.reshape(shape), ("z", "y", "x", "c"))
    return jax.shard_map(
        local,
        mesh=finer,
        in_specs=(
            P(SP, TP),
            P(),
            P(SP, TP),
            P(SP, TP),
            P(None, TP),
            P(TP),
            P(None, TP),
            P(SP, None),
            P(),
            P(SP, None),
            P(None, TP),
            P(None, TP),
            P(TP, None),
            P(TP, None),
        ),
        out_specs=(P((*SP, *TP), None), P(SP, TP)),
        check_vma=False,
    )
```

time: 381 us -> 93.4 us (0.25)
  waiting for transfers between devices: 249 us -> 0 us
  Pallas kernels: 0 us -> 91.1 us
  matrix products: 36.5 us -> 0 us
  blocking collectives: 31.7 us -> 0 us
  starting transfers between devices: 27.5 us -> 0 us
  between operations: 14.3 us -> 0.65 us
  other arithmetic: 13.3 us -> 0 us
  local copies, waits for them, and re-layouts: 7.75 us -> 1.49 us
    all_gather x2 -> x0, waiting for transfers between devices: 236 us -> none  [side_by_side(): result, at, done = (lax.all_gather(both, axis, axis=dim, tiled=True), 0, [])]
    pallas_call x0 -> x2, Pallas kernels: none -> 91.1 us  [the longest x1 90.4 us: local(): pl.pallas_call(functools.partial(layer, sizes), out_shape=[jax.ShapeDtype...]
    dot_general x10 -> x0, matrix products: 36.5 us -> none  [the longest x1 9.22 us: local(): jnp.einsum('thl,kl->thk', query_latent, latent_piece, preferred_element_t...]
    all_gather x4 -> x0, blocking collectives: 31.7 us -> none  [all_blocks(): parts = lax.all_gather(parts, axes[k], axis=0, tiled=True)]
    all_to_all x2 -> x0, starting transfers between devices: 26.2 us -> none  [the longest x1 14.6 us: sent_to_all(): return lax.all_to_all(copies, axis, split_axis=0, concat_axis=0, tiled=True)]
    all_to_all x2 -> x0, waiting for transfers between devices: 12.6 us -> none  [the longest x1 8.78 us: summed_on_arrival(): parts = lax.all_to_all(split_up(shard, dim, count), axis, 0, 0, tiled=True)]
    reduce_sum x5 -> x0, other arithmetic: 4.4 us -> none  [the longest x1 2.13 us: local(): running_sum = jnp.sum(weights, axis=-1)]
  transfers between devices with their start and end apart: 5 -> 0, of which waited for: 4 -> 0; matrix products, arithmetic and copies ran while one was open for 5% -> 0% of each run, Pallas kernels for 0% -> 0%
where the time goes in v2:
time: 93.4 us; the launch traced here: 93.2 us
  Pallas kernels  91.1 us (98%)
  local copies, waits for them, and re-layouts  1.49 us (2%)
    pallas_call x1, Pallas kernels, local(): pl.pallas_call(functools.partial(layer, sizes), out_shape=[jax.ShapeDtype...  90.4 us

profile of v2, /device:TPU:1, one launch (start us, length us, event | category | flops | bytes accessed | tf_op | source)
XLA Modules:
  0.0 93.2 jit_solution(781162731042818700)
XLA Ops:
  0.6 90.4 %layer.1 = (bf16[16,2048]{1,0:T(8,128)(2,1)}, f32[2,128]{1,0:T(2,128)}) custom-call(bf16[128,256]{1,0:T(8,128)(2,1)} %tok.1, bf16[32,256]{1,0:T(8,128)(2,1)} %wv.1, bf16[32,256]{1,0:T(8,128)(2,1)} %wg.1, bf16[32,512]{1,0:T(8,128)(2,1)} %wl.1, bf16[32,64]{1,0:T(8,128)(2,1)} %wr.1, f32[1,2048]{1,0:T(1,128)} %bitcast.4, f32[1,512]{1,0:T(1,128)} %bitcast.5, ...), custom_call_target="tpu_custom_call" | custom-call | tf_op jit(solution)/shard_map/layer/pallas_call | solution.py:753
  91.1 0.0 copy-start
  91.1 0.8 copy-done
  91.9 0.0 copy-start.1
  91.9 0.7 copy-done.1
  92.6 0.6 hand_on.1
Async XLA Ops:
  91.1 0.8 copy-start
  91.9 0.7 copy-start.1
